TPU v7x, 32 devices: a whole 2x2x4 slice. The times are simulated.
32 devices in a mesh: sp: 4 (over z), fs: 4 (over y, x), tp: 2 (over core).
Axes of the slice: x: 2, y: 2, z: 4, core: 2. Of those that a mesh axis runs over, the one named last changes fastest.
Arguments:
- tokens: bfloat16 [4, 1024, 2048], P('fs', 'sp'), may hold values from -6 to 6
- mix_gain: float32 [2048], replicated, may hold values from 0.1 to 1.9
- query_down: bfloat16 [2048, 768], P('fs', 'tp'), may hold values from -0.125 to 0.125
- memory_down: bfloat16 [2048, 512], P('fs', 'tp'), may hold values from -0.125 to 0.125
- rope_weight: bfloat16 [2048, 32], replicated, may hold values from -0.125 to 0.125
- query_up: bfloat16 [768, 1536], P('fs', 'tp'), may hold values from -0.21875 to 0.21875
- key_up: bfloat16 [512, 1024], P('fs', 'tp'), may hold values from -0.25 to 0.25
- value_up: bfloat16 [512, 1024], P('fs', 'tp'), may hold values from -0.25 to 0.25
- latent_gain: float32 [768], replicated, may hold values from 0.1 to 1.9
- memory_gain: float32 [512], replicated, may hold values from 0.1 to 1.9
- query_gain: float32 [96], replicated, may hold values from 1 to 16
- key_gain: float32 [96], replicated, may hold values from 0.1 to 1.9
- conv_value: bfloat16 [2048, 1024], P('fs', 'tp'), may hold values from -1 to 1
- conv_gate: bfloat16 [2048, 1024], P('fs', 'tp'), may hold values from -0.125 to 0.125
- conv_kernel: bfloat16 [31, 1024], P(None, 'tp'), may hold values from -50 to 50
- channel_gain: float32 [1024], P('tp'), may hold values from 0.1 to 1.9
- channel_shift: float32 [1024], P('tp'), may hold values from -3 to 3
- heads_out: bfloat16 [1024, 2048], P('tp', 'fs'), may hold values from -0.75 to 0.75
- conv_out: bfloat16 [1024, 2048], P('tp', 'fs'), may hold values from -0.1875 to 0.1875
Outputs:
- mixed: bfloat16 [4, 1024, 2048], P('fs', 'sp')
All inputs are finite; a program needn't handle non-finite values.
Results may differ from a plain program's by a relative error of at most 0.015.
The roundings to bfloat16 on the way count: a program that leaves them out, or rounds other values in their place, can miss the bound.
Values may be sent and summed in bfloat16 or wider, within the bound.
A program may use at most 64 MiB of HBM per device.

v0:
```python
import jax
import jax.numpy as jnp
from jax import lax
from jax.sharding import PartitionSpec as P

QK_NOPE = 64
QK_ROPE = 32
V_DIM = 64
CONV_W = 1024
SEG = 64
QK_DIM = 96


epsilon = 1e-06
rope_base = 10000.0
masked_score = -1e30


def from_behind(value, axis, by):
    count = lax.axis_size(axis)
    pairs = [(i, i + by) for i in range(count) if 0 <= i + by < count]
    return lax.ppermute(value, axis, pairs)


def norm_rows(matrix, scale_vector):
    return (
        matrix
        * lax.rsqrt(jnp.mean(matrix * matrix, axis=-1, keepdims=True) + epsilon)
        * scale_vector
    )


def rope_tables(positions):
    inverse_freq = 1.0 / rope_base ** (jnp.arange(0, QK_ROPE, 2, dtype=jnp.float32) / QK_ROPE)
    angles = positions.astype(jnp.float32)[:, None] * inverse_freq[None, :]
    return (jnp.cos(angles)[:, None, :], jnp.sin(angles)[:, None, :])


def rotate(matrix, cosine_table, sine_table):
    half_width = matrix.shape[-1] // 2
    front_half = matrix[..., :half_width]
    back_half = matrix[..., half_width:]
    return jnp.concatenate(
        [
            front_half * cosine_table - back_half * sine_table,
            front_half * sine_table + back_half * cosine_table,
        ],
        axis=-1,
    )


def heads_query(latent, weight, scale_vector, cosine_table, sine_table):
    row_count = latent.shape[0]
    projected = jnp.dot(latent, weight, preferred_element_type=jnp.float32)
    projected = norm_rows(
        projected.reshape(row_count, weight.shape[1] // QK_DIM, QK_DIM), scale_vector
    )
    turned = rotate(projected[..., QK_NOPE:], cosine_table, sine_table)
    return jnp.concatenate([projected[..., :QK_NOPE], turned], axis=-1).astype(jnp.bfloat16)


def heads_key(latent, rope_rows, weight, scale_vector, cosine_table, sine_table):
    row_count = latent.shape[0]
    head_count = weight.shape[1] // QK_NOPE
    nope_part = jnp.dot(latent, weight, preferred_element_type=jnp.float32).reshape(
        row_count, head_count, QK_NOPE
    )
    shared = jnp.broadcast_to(
        rope_rows.astype(jnp.float32)[:, None, :], (row_count, head_count, QK_ROPE)
    )
    joined = norm_rows(jnp.concatenate([nope_part, shared], axis=-1), scale_vector)
    turned = rotate(joined[..., QK_NOPE:], cosine_table, sine_table)
    return jnp.concatenate([joined[..., :QK_NOPE], turned], axis=-1).astype(jnp.bfloat16)


def depthwise(extended, kernel, row_count):

    def add_tap(tap_index, running):
        window = lax.dynamic_slice_in_dim(extended, tap_index, row_count, 0).astype(jnp.float32)
        weight_row = lax.dynamic_slice_in_dim(kernel, tap_index, 1, 0).astype(jnp.float32)
        return running + window * weight_row

    return lax.fori_loop(
        0, kernel.shape[0], add_tap, jnp.zeros((row_count, kernel.shape[1]), jnp.float32)
    )


def key_block(key_count):
    block_size = key_count
    while block_size > 2048 and block_size % 2 == 0:
        block_size = block_size // 2
    return block_size


def local(
    tokens,
    mix_gain,
    query_down,
    memory_down,
    rope_weight,
    query_up,
    key_up,
    value_up,
    latent_gain,
    memory_gain,
    query_gain,
    key_gain,
    conv_value,
    conv_gate,
    conv_kernel,
    channel_gain,
    channel_shift,
    heads_out,
    conv_out,
):
    own_rows = tokens[0]
    normed = norm_rows(own_rows.astype(jnp.float32), mix_gain).astype(jnp.bfloat16)
    down_query, down_memory, conv_values, conv_gates, up_query, up_keys, up_values = (
        lax.all_gather(query_down, "fs", axis=0, tiled=True),
        lax.all_gather(memory_down, "fs", axis=0, tiled=True),
        lax.all_gather(conv_value, "fs", axis=0, tiled=True),
        lax.all_gather(conv_gate, "fs", axis=0, tiled=True),
        lax.all_gather(query_up, "fs", axis=0, tiled=True),
        lax.all_gather(key_up, "fs", axis=0, tiled=True),
        lax.all_gather(value_up, "fs", axis=0, tiled=True),
    )
    out_heads, out_conv = (
        lax.all_gather(heads_out, "fs", axis=1, tiled=True),
        lax.all_gather(conv_out, "fs", axis=1, tiled=True),
    )
    joined = jnp.concatenate(
        [down_query, down_memory, rope_weight, conv_values, conv_gates], axis=1
    )
    query_cols = down_query.shape[1]
    memory_cols = down_memory.shape[1]
    conv_cols = conv_values.shape[1]
    projected = jnp.dot(normed, joined, preferred_element_type=jnp.float32)
    row_count = projected.shape[0]
    rope_start = query_cols + memory_cols
    value_start = rope_start + QK_ROPE
    latent_query = projected[:, :query_cols].astype(jnp.bfloat16)
    latent_memory = projected[:, query_cols:rope_start].astype(jnp.bfloat16)
    rope_rows = projected[:, rope_start:value_start].astype(jnp.bfloat16)
    gated = (
        projected[:, value_start : value_start + conv_cols]
        * jax.nn.sigmoid(projected[:, value_start + conv_cols :])
    ).astype(jnp.bfloat16)
    whole_query, whole_memory = (
        lax.all_gather(latent_query, "tp", axis=1, tiled=True),
        lax.all_gather(latent_memory, "tp", axis=1, tiled=True),
    )
    query_normed = norm_rows(whole_query.astype(jnp.float32), latent_gain).astype(jnp.bfloat16)
    memory_normed = norm_rows(whole_memory.astype(jnp.float32), memory_gain).astype(jnp.bfloat16)
    positions = lax.axis_index("sp") * row_count + jnp.arange(row_count, dtype=jnp.int32)
    cosine_table, sine_table = rope_tables(positions)
    queries = heads_query(query_normed, up_query, query_gain, cosine_table, sine_table)
    head_count = queries.shape[1]
    query_segment = positions // SEG
    score_scale = QK_DIM ** (-0.5)
    tap_count = conv_kernel.shape[0]
    left_rim = from_behind(gated[row_count - (tap_count - 1) :], "sp", 1)
    conv_sum = depthwise(jnp.concatenate([left_rim, gated], axis=0), conv_kernel, row_count)
    row_sums, row_squares = lax.psum(
        (jnp.sum(conv_sum, axis=1), jnp.sum(conv_sum * conv_sum, axis=1)), "tp"
    )
    row_mean = row_sums / CONV_W
    spread = row_squares / CONV_W - row_mean * row_mean
    centered = conv_sum - row_mean[:, None]
    conv_result = jax.nn.silu(
        centered * lax.rsqrt(spread[:, None] + epsilon) * channel_gain + channel_shift
    ).astype(jnp.bfloat16)

    def attend(state_carry, key_rows, value_rows, key_pos):
        running_max, row_total, weighted = state_carry
        scores = (
            jnp.einsum("qhd,khd->qhk", queries, key_rows, preferred_element_type=jnp.float32)
            * score_scale
        )
        allowed = ((key_pos // SEG)[None, :] <= query_segment[:, None])[:, None, :]
        scores = jnp.where(allowed, scores, masked_score)
        new_max = jnp.maximum(running_max, jnp.max(scores, axis=2))
        weights = jnp.where(allowed, jnp.exp(scores - new_max[:, :, None]), 0.0)
        factor = jnp.exp(running_max - new_max)
        row_total = row_total * factor + jnp.sum(weights, axis=2)
        weighted = weighted * factor[:, :, None] + jnp.einsum(
            "qhk,khd->qhd",
            weights.astype(jnp.bfloat16),
            value_rows,
            preferred_element_type=jnp.float32,
        )
        return (new_max, row_total, weighted)

    initial = (
        jnp.full((row_count, head_count), masked_score, jnp.float32),
        jnp.zeros((row_count, head_count), jnp.float32),
        jnp.zeros((row_count, head_count, V_DIM), jnp.float32),
    )
    memory_piece = lax.all_gather(memory_normed, "sp", axis=0, tiled=True)
    rope_piece = lax.all_gather(rope_rows, "sp", axis=0, tiled=True)

    def block_keys(block_start, block_size):
        memory_block = lax.dynamic_slice_in_dim(memory_piece, block_start, block_size, 0)
        rope_block = lax.dynamic_slice_in_dim(rope_piece, block_start, block_size, 0)
        key_pos = block_start + jnp.arange(block_size, dtype=jnp.int32)
        cosine_keys, sine_keys = rope_tables(key_pos)
        key_rows = heads_key(memory_block, rope_block, up_keys, key_gain, cosine_keys, sine_keys)
        value_rows = (
            jnp.dot(memory_block, up_values, preferred_element_type=jnp.float32)
            .astype(jnp.bfloat16)
            .reshape(block_size, head_count, V_DIM)
        )
        return (key_rows, value_rows, key_pos)

    key_count = memory_piece.shape[0]
    block_size = key_block(key_count)

    def step(block_index, running):
        key_rows, value_rows, key_pos = block_keys(block_index * block_size, block_size)
        return attend(running, key_rows, value_rows, key_pos)

    final_state = lax.fori_loop(0, key_count // block_size, step, initial)
    running_max, row_total, weighted = final_state
    attention = (
        (weighted / row_total[:, :, None])
        .astype(jnp.bfloat16)
        .reshape(row_count, head_count * V_DIM)
    )
    mixer_rows = jnp.concatenate([attention, conv_result], axis=1)
    out_weight = jnp.concatenate([out_heads, out_conv], axis=0)
    partial_sum = jnp.dot(mixer_rows, out_weight, preferred_element_type=jnp.float32)
    mixed = lax.psum(partial_sum.astype(jnp.bfloat16), "tp")
    return mixed[None]


def solution(mesh):
    in_specs = (
        P("fs", "sp", None),
        P(),
        P("fs", "tp"),
        P("fs", "tp"),
        P(),
        P("fs", "tp"),
        P("fs", "tp"),
        P("fs", "tp"),
        P(),
        P(),
        P(),
        P(),
        P("fs", "tp"),
        P("fs", "tp"),
        P(None, "tp"),
        P("tp"),
        P("tp"),
        P("tp", "fs"),
        P("tp", "fs"),
    )
    out_specs = P("fs", "sp", None)
    return jax.shard_map(local, mesh=mesh, in_specs=in_specs, out_specs=out_specs, check_vma=False)
```

profile of v0, /device:TPU:0, one launch (start us, length us, event | category | flops | bytes accessed | tf_op | source)
XLA Modules:
  0.0 312.9 jit_solution(17738299763374971849)
XLA Ops:
  6.5 0.7 all-gather.11.cloned.1.call-update
  10.0 1.2 copy.25
  11.5 27.0 %all-gather.11.cloned.1.call-done = bf16[2048,256]{1,0:T(8,128)(2,1)} async-done(((bf16[512,256]{1,0:T(8,128)(2,1)}), bf16[2048,256]{1,0:T(8,128)(2,1)}) %all-gather.11.cloned.1.call-update) | async-done | bytes 1048592 | tf_op jit(solution)/shard_map/all_gather | solution.py:120
  38.4 32.7 %all-gather.9.cloned.1.call-done = bf16[2048,384]{1,0:T(8,128)(2,1)} async-done(((bf16[512,384]{1,0:T(8,128)(2,1)}), bf16[2048,384]{1,0:T(8,128)(2,1)}) %all-gather.9.cloned.1.call-update) | async-done | bytes 1572880 | tf_op jit(solution)/shard_map/all_gather | solution.py:119
  71.1 37.1 %all-gather.13.cloned.1.call-done = bf16[2048,512]{1,0:T(8,128)(2,1)} async-done(((bf16[512,512]{1,0:T(8,128)(2,1)}), bf16[2048,512]{1,0:T(8,128)(2,1)}) %all-gather.13.cloned.1.call-update) | async-done | bytes 2097168 | tf_op jit(solution)/shard_map/all_gather | solution.py:121
  108.2 36.9 %all-gather.15.cloned.1.call-done = bf16[2048,512]{1,0:T(8,128)(2,1)} async-done(((bf16[512,512]{1,0:T(8,128)(2,1)}), bf16[2048,512]{1,0:T(8,128)(2,1)}) %all-gather.15.cloned.1.call-update) | async-done | bytes 2097168 | tf_op jit(solution)/shard_map/all_gather | solution.py:122
  145.1 12.6 %concatenate.25 = bf16[2048,1696]{1,0:T(8,128)(2,1)} concatenate(bf16[2048,384]{1,0:T(8,128)(2,1)} %all-gather.9.cloned.1.call-done, bf16[2048,256]{1,0:T(8,128)(2,1)} %all-gather.11.cloned.1.call-done, bf16[2048,32]{1,0:T(8,128)(2,1)S(1)} %copy.25, bf16[2048,512]{1,0:T(8,128)(2,1)} %all-gather.13.cloned.1.call-done, bf16[2048,512]{1,0:T(8,128)(2,1)} %all-gather.15.cloned.1.call-done), dimensions={1} | concatenate | bytes 13893632 | tf_op jit(solution)/shard_map/concatenate | solution.py:131
  157.7 7.4 %fusion.76 = (bf16[256,1696]{0,1:T(8,128)(2,1)S(1)}, f32[256,1696]{0,1:T(8,128)}) fusion(bf16[2048,1696]{1,0:T(8,128)(2,1)} %concatenate.25, bf16[1,256,2048]{2,1,0:T(8,128)(2,1)S(1)} %copy-done.1, f32[2048]{0:T(1024)S(1)} %copy-done.11, f32[256]{0:T(256)S(1)} %add_rsqrt_fusion.5), kind=kOutput, calls=%fused_computation.113 | convolution fusion | flops 1780916224 | bytes 10609664 | tf_op jit(solution)/shard_map/dot_general | solution.py:137
  165.1 2.1 all_gather.43
  167.3 0.9 fusion.47
  168.3 0.7 all-gather.21.cloned.1.call-update
  169.0 0.7 all-gather.23.cloned.1.call-update
  169.9 10.3 %all_gather.45 = bf16[512,512]{1,0:T(8,128)(2,1)S(1)} all-gather(bf16[128,512]{1,0:T(8,128)(2,1)S(1)} %copy-done.3), channel_id=1, replica_groups=mesh['sp'=4,'fs'=4,'tp'=2] {'fs'}, dimensions={0}, use_global_device_ids=true | all-gather | bytes 655360 | tf_op jit(solution)/shard_map/all_gather | solution.py:124
  180.6 9.1 %all_gather.49 = bf16[512,512]{1,0:T(8,128)(2,1)S(1)} all-gather(bf16[128,512]{1,0:T(8,128)(2,1)S(1)} %copy-done.4), channel_id=1, replica_groups=mesh['sp'=4,'fs'=4,'tp'=2] {'fs'}, dimensions={0}, use_global_device_ids=true | all-gather | bytes 655360 | tf_op jit(solution)/shard_map/all_gather | solution.py:125
  189.9 0.9 slice.68
  190.8 2.1 all_gather.47
  193.1 2.0 fusion.56
  195.2 1.3 fusion.55
  196.6 3.4 %collective-permute-start = (bf16[30,512]{0,1:T(8,128)(2,1)S(1)}, bf16[30,512]{0,1:T(8,128)(2,1)S(1)}, u32[]{:S(2)}, u32[]{:S(2)}) collective-permute-start(bf16[30,512]{0,1:T(8,128)(2,1)S(1)} %slice.74), channel_id=1, source_target_pairs={{0,8},{8,16},{16,24},{1,9},{9,17},{17,25},{2,10},{10,18},{18,26},{... | collective-permute-start | bytes 92168 | tf_op jit(solution)/shard_map/ppermute | solution.py:22
  200.3 0.7 slice.64
  201.0 13.2 %all_gather.46 = bf16[1024,32]{0,1:T(8,128)(2,1)S(1)} all-gather(bf16[256,32]{0,1:T(8,128)(2,1)S(1)} %slice.64), channel_id=1, replica_groups=mesh['sp'=4,'fs'=4,'tp'=2] {'sp'}, dimensions={0}, use_global_device_ids=true | all-gather | bytes 81920 | tf_op jit(solution)/shard_map/all_gather | solution.py:199
  214.4 38.2 %while.9 = (s32[]{:T(128)}, f32[256,512]{1,0:T(8,128)S(1)}, bf16[286,512]{0,1:T(8,128)(2,1)S(1)}, bf16[31,512]{1,0:T(8,128)(2,1)}, s32[]{:T(128)}, /*index=5*/s32[]{:T(128)}) while((s32[]{:T(128)}, f32[256,512]{1,0:T(8,128)S(1)}, bf16[286,512]{0,1:T(8,128)(2,1)S(1)}, bf16[31,512]{1,0:T(8,128)(2,1)}, s32[]{:T(128)}, ...), condition=%wide.region_8.9_spmd.clone, body=%wide.region_7.8_spmd.clone.sunk | while | flops 524803 | bytes 2364503 | solution.py:83
  214.7 0.7 dynamic-slice_convert_fusion.2
  216.0 0.7 dynamic-slice_convert_fusion.2
  217.2 0.7 dynamic-slice_convert_fusion.2
  218.4 0.7 dynamic-slice_convert_fusion.2
  219.7 0.7 dynamic-slice_convert_fusion.2
  220.9 0.7 dynamic-slice_convert_fusion.2
  222.1 0.7 dynamic-slice_convert_fusion.2
  223.4 0.7 dynamic-slice_convert_fusion.2
  224.6 0.7 dynamic-slice_convert_fusion.2
  225.8 0.7 dynamic-slice_convert_fusion.2
  227.1 0.7 dynamic-slice_convert_fusion.2
  228.3 0.7 dynamic-slice_convert_fusion.2
  229.5 0.7 dynamic-slice_convert_fusion.2
  230.8 0.7 dynamic-slice_convert_fusion.2
  232.0 0.7 dynamic-slice_convert_fusion.2
  233.2 0.7 dynamic-slice_convert_fusion.2
  234.4 0.7 dynamic-slice_convert_fusion.2
  235.7 0.7 dynamic-slice_convert_fusion.2
  236.9 0.7 dynamic-slice_convert_fusion.2
  238.1 0.7 dynamic-slice_convert_fusion.2
  239.4 0.7 dynamic-slice_convert_fusion.2
  240.6 0.7 dynamic-slice_convert_fusion.2
  241.8 0.7 dynamic-slice_convert_fusion.2
  243.1 0.7 dynamic-slice_convert_fusion.2
  244.3 0.7 dynamic-slice_convert_fusion.2
  245.5 0.7 dynamic-slice_convert_fusion.2
  246.8 0.7 dynamic-slice_convert_fusion.2
  248.0 0.7 dynamic-slice_convert_fusion.2
  249.2 0.7 dynamic-slice_convert_fusion.2
  250.5 0.7 dynamic-slice_convert_fusion.2
  251.7 0.7 dynamic-slice_convert_fusion.2
  253.0 2.7 all-reduce
  255.9 2.0 fusion.77
  258.5 0.8 multiply_multiply_fusion
  259.6 1.7 fusion
  261.3 2.0 fusion.1
  263.3 0.8 convolution_convert_fusion
  264.1 2.2 fusion.39
  266.3 13.7 %all-gather.23.cloned.1.call-done = bf16[512,2048]{1,0:T(8,128)(2,1)} async-done(((bf16[512,512]{1,0:T(8,128)(2,1)}), bf16[512,2048]{1,0:T(8,128)(2,1)}) %all-gather.23.cloned.1.call-update) | async-done | bytes 2097168 | tf_op jit(solution)/shard_map/all_gather | solution.py:129
  280.0 4.5 %fusion.13 = bf16[1,256,2048]{2,1,0:T(8,128)(2,1)} fusion(bf16[512,2048]{1,0:T(8,128)(2,1)} %all-gather.23.cloned.1.call-done, bf16[512,2048]{1,0:T(8,128)(2,1)} %all-gather.21.cloned.1.call-done, bf16[256,512]{0,1:T(8,128)(2,1)S(1)} %multiply_convert_fusion, bf16[256,512]{0,1:T(8,128)(2,1)S(1)} %bitcast.58), kind=kOutput, calls=%fused_computation.20 | convolution fusion | flops 1083703296 | bytes 5767168 | tf_op jit(solution)/shard_map/dot_general | solution.py:230
  284.5 19.6 %all-reduce.3.cloned.1.call-done = bf16[1,256,2048]{2,1,0:T(8,128)(2,1)} async-done(((bf16[1,256,2048]{2,1,0:T(8,128)(2,1)}), bf16[1,256,2048]{2,1,0:T(8,128)(2,1)}) %all-reduce.3.cloned.1.call-update) | async-done | bytes 1048592 | tf_op jit(solution)/shard_map/psum | solution.py:231
  304.1 2.3 copy.42
  (170 shorter events, 21.4 us)
Async XLA Ops:
  6.5 4.6 %copy-start.1 = (bf16[1,256,2048]{2,1,0:T(8,128)(2,1)S(1)}, bf16[1,256,2048]{2,1,0:T(8,128)(2,1)}, u32[]{:S(2)}) copy-start(bf16[1,256,2048]{2,1,0:T(8,128)(2,1)} %param.21) | copy-start | bytes 3145732
  6.5 31.9 %all-gather.11.cloned.1.call-start = ((), (), s32[]{:S(2)}) async-start(), calls=%async_computation.1 | async-start | bytes 1310720 | tf_op jit(solution)/shard_map/all_gather | solution.py:120
  7.3 63.9 %all-gather.9.cloned.1.call-start = ((), (), s32[]{:S(2)}) async-start(), calls=%async_computation | async-start | bytes 1966080 | tf_op jit(solution)/shard_map/all_gather | solution.py:119
  8.0 100.2 %all-gather.13.cloned.1.call-start = ((), (), s32[]{:S(2)}) async-start(), calls=%async_computation.2 | async-start | bytes 2621440 | tf_op jit(solution)/shard_map/all_gather | solution.py:121
  8.7 136.4 %all-gather.15.cloned.1.call-start = ((), (), s32[]{:S(2)}) async-start(), calls=%async_computation.3 | async-start | bytes 2621440 | tf_op jit(solution)/shard_map/all_gather | solution.py:122
  9.3 183.8 %all-gather.19.cloned.1.call-start = ((), (), s32[]{:S(2)}) async-start(), calls=%async_computation.5 | async-start | bytes 1474560 | tf_op jit(solution)/shard_map/all_gather | solution.py:123
  9.9 246.0 %all-gather.17.cloned.1.call-start = ((), (), s32[]{:S(2)}) async-start(), calls=%async_computation.4 | async-start | bytes 1310720 | tf_op jit(solution)/shard_map/all_gather | solution.py:198
  11.4 146.3 %copy-start.11 = (f32[2048]{0:T(1024)S(1)}, f32[2048]{0:T(1024)}, u32[]{:S(2)}) copy-start(f32[2048]{0:T(1024)} %param.22) | copy-start | bytes 24580
  157.7 9.6 %copy-start.6 = (f32[512]{0:T(512)S(1)}, f32[512]{0:T(512)}, u32[]{:S(2)}) copy-start(f32[512]{0:T(512)} %param.30) | copy-start | bytes 6148
  157.7 12.2 %copy-start.3 = (bf16[128,512]{1,0:T(8,128)(2,1)S(1)}, bf16[128,512]{1,0:T(8,128)(2,1)}, u32[]{:S(2)}) copy-start(bf16[128,512]{1,0:T(8,128)(2,1)} %param.27) | copy-start | bytes 393220
  165.1 2.1 copy-start.2
  165.1 15.5 %copy-start.4 = (bf16[128,512]{1,0:T(8,128)(2,1)S(1)}, bf16[128,512]{1,0:T(8,128)(2,1)}, u32[]{:S(2)}) copy-start(bf16[128,512]{1,0:T(8,128)(2,1)} %param.28) | copy-start | bytes 393220
  165.1 28.0 %copy-start.5 = (f32[768]{0:T(1024)S(1)}, f32[768]{0:T(1024)}, u32[]{:S(2)}) copy-start(f32[768]{0:T(1024)} %param.29) | copy-start | bytes 9220
  168.2 98.1 %all-gather.21.cloned.1.call-start = ((), (), s32[]{:S(2)}) async-start(), calls=%async_computation.6 | async-start | bytes 2621440 | tf_op jit(solution)/shard_map/all_gather | solution.py:128
  169.0 111.0 %all-gather.23.cloned.1.call-start = ((), (), s32[]{:S(2)}) async-start(), calls=%async_computation.7 | async-start | bytes 2621440 | tf_op jit(solution)/shard_map/all_gather | solution.py:129
  169.7 134.3 %all-reduce.3.cloned.1.call-start = ((), (), s32[]{:S(2)}) async-start(), calls=%async_computation.8 | async-start | bytes 2097152 | tf_op jit(solution)/shard_map/psum | solution.py:231
  189.7 10.4 %copy-start.9 = (f32[96]{0:T(128)S(1)}, f32[96]{0:T(128)}, u32[]{:S(2)}) copy-start(f32[96]{0:T(128)} %param.31) | copy-start | bytes 1156
  196.6 17.5 %collective-permute-start = (bf16[30,512]{0,1:T(8,128)(2,1)S(1)}, bf16[30,512]{0,1:T(8,128)(2,1)S(1)}, u32[]{:S(2)}, u32[]{:S(2)}) collective-permute-start(bf16[30,512]{0,1:T(8,128)(2,1)S(1)} %slice.74), channel_id=1, source_target_pairs={{0,8},{8,16},{16,24},{1,9},{9,17},{17,25},{2,10},{10,18},{18,26},{... | collective-permute-start | bytes 92168 | tf_op jit(solution)/shard_map/ppermute | solution.py:22
  214.4 41.3 %copy-start.7 = (f32[512]{0:T(512)S(1)}, f32[512]{0:T(512)}, u32[]{:S(2)}) copy-start(f32[512]{0:T(512)} %param.37) | copy-start | bytes 6148
  214.4 41.2 %copy-start.8 = (f32[512]{0:T(512)S(1)}, f32[512]{0:T(512)}, u32[]{:S(2)}) copy-start(f32[512]{0:T(512)} %param.36) | copy-start | bytes 6148
  255.9 2.6 copy-start.10
  261.3 2.1 copy-start
Sparse Core Ops, SparseCore 0:
  9.2 29.2 all-gather.10
  40.3 30.8 all-gather.8
  73.0 35.1 all-gather.12
  109.9 35.1 all-gather.14
  146.8 27.6 all-gather.18
  175.9 30.1 all-gather.16
  208.0 35.0 all-gather.20
  244.9 35.0 all-gather.22
  284.6 19.4 all-reduce.2
where the time goes:
time: 315 us; the launch traced here: 313 us
  waiting for transfers between devices  172 us (55%)
  blocking collectives  39.4 us (13%)
  other arithmetic  35.9 us (11%)
  local copies, waits for them, and re-layouts  27.4 us (9%)
  matrix products  20.4 us (6%)
  between operations  13.6 us (4%)
  starting transfers between devices  3.7 us (1%)
    all_gather x1, waiting for transfers between devices, local(): lax.all_gather(conv_value, 'fs', axis=0, tiled=True)  37.1 us
    all_gather x1, waiting for transfers between devices, local(): lax.all_gather(conv_gate, 'fs', axis=0, tiled=True)  36.9 us
    all_gather x1, waiting for transfers between devices, local(): lax.all_gather(query_down, 'fs', axis=0, tiled=True)  32.7 us
    all_gather x1, waiting for transfers between devices, local(): lax.all_gather(memory_down, 'fs', axis=0, tiled=True)  27 us
    mul x31, other arithmetic, add_tap(): return running + window * weight_row  22 us
    psum x1, waiting for transfers between devices, local(): mixed = lax.psum(partial_sum.astype(jnp.bfloat16), 'tp')  19.6 us
    all_gather x1, waiting for transfers between devices, local(): lax.all_gather(conv_out, 'fs', axis=1, tiled=True)  13.7 us
    all_gather x1, blocking collectives, local(): rope_piece = lax.all_gather(rope_rows, 'sp', axis=0, tiled=True)  13.2 us
  transfers between devices with their start and end apart: 10, of which 6 were waited for; matrix products, arithmetic and copies ran while one was open for 25% of the time, Pallas kernels for 0%

commit v1 on v0

--- a/solution.py
+++ b/solution.py
@@ -1,7 +1,13 @@
+import functools
+
 import jax
 import jax.numpy as jnp
 from jax import lax
+from jax.experimental import pallas as pl
+from jax.experimental.pallas import tpu as pltpu
 from jax.sharding import PartitionSpec as P
+
+MESH_ID = pl.DeviceIdType.MESH
 
 QK_NOPE = 64
 QK_ROPE = 32
@@ -14,12 +20,6 @@
 epsilon = 1e-06
 rope_base = 10000.0
 masked_score = -1e30
-
-
-def from_behind(value, axis, by):
-    count = lax.axis_size(axis)
-    pairs = [(i, i + by) for i in range(count) if 0 <= i + by < count]
-    return lax.ppermute(value, axis, pairs)
 
 
 def norm_rows(matrix, scale_vector):
@@ -73,16 +73,237 @@
     return jnp.concatenate([joined[..., :QK_NOPE], turned], axis=-1).astype(jnp.bfloat16)
 
 
-def depthwise(extended, kernel, row_count):
-
-    def add_tap(tap_index, running):
-        window = lax.dynamic_slice_in_dim(extended, tap_index, row_count, 0).astype(jnp.float32)
-        weight_row = lax.dynamic_slice_in_dim(kernel, tap_index, 1, 0).astype(jnp.float32)
-        return running + window * weight_row
-
-    return lax.fori_loop(
-        0, kernel.shape[0], add_tap, jnp.zeros((row_count, kernel.shape[1]), jnp.float32)
-    )
+RIM = 32
+
+
+def relayed_rows(rows, paired):
+    return (rows * 3 // 8) // 16 * 16 if paired else 0
+
+
+def gather_kernel(
+    sizes,
+    x_ref, gain_ref, rope_ref, taps_ref,
+    qd, md, cv, cg, qu, ku, vu, ho, co,
+    lq_ref, lm_ref, rr_ref, sum_ref, qu_all, ku_all, vu_all, ho_all, co_all,
+    qd_all, md_all, cv_all, cg_all, normed, acc_q, acc_v, acc_g, ext, tail, rim,
+    send_a, recv_a, send_z, recv_z, local_sem, rim_sem,
+):
+    n_fs, n_sp = sizes
+    paired = n_sp % 2 == 0
+    f = lax.axis_index("fs")
+    s = lax.axis_index("sp")
+    parity = lax.rem(s, 2)
+    partner = s + 1 - 2 * parity
+
+    barrier = pltpu.get_barrier_semaphore()
+    for k in range(1, n_fs):
+        pl.semaphore_signal(
+            barrier, inc=1, device_id={"fs": lax.rem(f + k, n_fs)}, device_id_type=MESH_ID
+        )
+
+    beside = sorted({1 % n_sp, (n_sp - 1) % n_sp} - {0})
+    for step in beside:
+        pl.semaphore_signal(
+            barrier, inc=1, device_id={"sp": lax.rem(s + step, n_sp)}, device_id_type=MESH_ID
+        )
+    pl.semaphore_wait(barrier, n_fs - 1 + len(beside))
+
+    jobs = [
+        (qd, qd_all, 0), (md, md_all, 0), (cv, cv_all, 0), (cg, cg_all, 0),
+        (qu, qu_all, 0), (ku, ku_all, 0), (vu, vu_all, 0), (ho, ho_all, 1), (co, co_all, 1),
+    ]
+
+    def place(whole, shard, dim, owner, start, count):
+        rows, cols = shard.shape
+        if dim == 0:
+            return whole.at[pl.ds(pl.multiple_of(owner * rows + start, 16), count), :]
+        return whole.at[
+            pl.ds(pl.multiple_of(start, 16), count),
+            pl.ds(pl.multiple_of(owner * cols, 128), cols),
+        ]
+
+    first, relay, own = [], [], []
+    for a, (shard, whole, dim) in enumerate(jobs):
+        rows = shard.shape[0]
+        less = relayed_rows(rows, paired)
+        start = parity * less
+        for k in range(1, n_fs):
+            copy = pltpu.make_async_remote_copy(
+                src_ref=shard.at[pl.ds(pl.multiple_of(start, 16), rows - less), :],
+                dst_ref=place(whole, shard, dim, f, start, rows - less),
+                send_sem=send_a.at[a, k - 1],
+                recv_sem=recv_a.at[a, k - 1],
+                device_id={"fs": lax.rem(f + k, n_fs)},
+                device_id_type=MESH_ID,
+            )
+            copy.start()
+            first.append(copy)
+            if less:
+                lack = parity * (rows - less)
+                owner = lax.rem(f + n_fs - k, n_fs)
+                relay.append(pltpu.make_async_remote_copy(
+                    src_ref=place(whole, shard, dim, owner, lack, less),
+                    dst_ref=place(whole, shard, dim, owner, lack, less),
+                    send_sem=send_z.at[a, k - 1],
+                    recv_sem=recv_z.at[a, k - 1],
+                    device_id={"sp": partner},
+                    device_id_type=MESH_ID,
+                ))
+        mine = pltpu.make_async_copy(
+            shard, place(whole, shard, dim, f, 0, rows), local_sem.at[a]
+        )
+        mine.start()
+        own.append(mine)
+
+    rows = x_ref.shape[0]
+    part = 32
+
+    @pl.loop(0, rows // part)
+    def _(i):
+        at = pl.ds(pl.multiple_of(i * part, part), part)
+        x = x_ref[at, :].astype(jnp.float32)
+        scale = lax.rsqrt(jnp.mean(x * x, axis=-1, keepdims=True) + epsilon)
+        normed[at, :] = (x * scale * gain_ref[...]).astype(jnp.bfloat16)
+
+    per = n_fs - 1
+
+    def pass_on(a):
+        for k in range(per):
+            first[a * per + k].wait_recv()
+            if paired:
+                relay[a * per + k].start()
+
+    def complete(a):
+        own[a].wait()
+        if paired:
+            for k in range(per):
+                relay[a * per + k].wait_recv()
+
+    depth = qd.shape[0]
+
+    def project(weight, acc):
+        acc[...] = jnp.zeros_like(acc)
+
+        @pl.loop(0, n_fs)
+        def _(i):
+            at = pl.ds(pl.multiple_of(i * depth, depth), depth)
+            acc[...] += jnp.dot(
+                normed[:, at], weight[at, :], preferred_element_type=jnp.float32
+            )
+
+    rr_ref[...] = jnp.dot(
+        normed[...], rope_ref[...], preferred_element_type=jnp.float32
+    ).astype(jnp.bfloat16)
+    pass_on(0)
+    pass_on(1)
+    complete(0)
+    project(qd_all, acc_q)
+    lq_ref[...] = acc_q[...].astype(jnp.bfloat16)
+    pass_on(2)
+    complete(1)
+    acc_m = acc_q.at[:, pl.ds(0, md.shape[1])]
+    project(md_all, acc_m)
+    lm_ref[...] = acc_m[...].astype(jnp.bfloat16)
+    pass_on(3)
+    complete(2)
+    project(cv_all, acc_v)
+    pass_on(4)
+    complete(3)
+    project(cg_all, acc_g)
+    pass_on(5)
+
+    @pl.loop(0, rows // part)
+    def _(i):
+        at = pl.ds(pl.multiple_of(i * part, part), part)
+        gated = (acc_v[at, :] * jax.nn.sigmoid(acc_g[at, :])).astype(jnp.bfloat16)
+        ext[pl.ds(pl.multiple_of(RIM + i * part, part), part), :] = gated.astype(jnp.float32)
+
+    tail[...] = ext[pl.ds(rows, RIM), :].astype(jnp.bfloat16)
+    rim_copy = pltpu.make_async_remote_copy(
+        src_ref=tail, dst_ref=rim, send_sem=rim_sem.at[0], recv_sem=rim_sem.at[1],
+        device_id={"sp": lax.rem(s + 1, n_sp)}, device_id_type=MESH_ID,
+    )
+
+    @pl.when(s < n_sp - 1)
+    def _():
+        rim_copy.start()
+
+    pass_on(6)
+
+    @pl.when(s > 0)
+    def _():
+        rim_copy.wait_recv()
+        ext[pl.ds(0, RIM), :] = rim[...].astype(jnp.float32)
+
+    @pl.when(s == 0)
+    def _():
+        ext[pl.ds(0, RIM), :] = jnp.zeros((RIM, ext.shape[1]), jnp.float32)
+
+    pass_on(7)
+    tap_count = taps_ref.shape[0]
+    block = 64
+
+    @pl.loop(0, ext.shape[1] // 128)
+    def _(c):
+        cols = pl.ds(pl.multiple_of(c * 128, 128), 128)
+        taps = taps_ref[:, cols].astype(jnp.float32)
+        for r in range(0, rows, block):
+            total = jnp.zeros((block, 128), jnp.float32)
+            for j in range(tap_count):
+                total = total + ext[
+                    pl.ds(r + RIM - (tap_count - 1) + j, block), cols
+                ] * taps[j : j + 1, :]
+            sum_ref[pl.ds(r, block), cols] = total
+
+    pass_on(8)
+    for a in range(4, 9):
+        complete(a)
+    for copy in first + relay:
+        copy.wait_send()
+
+    @pl.when(s < n_sp - 1)
+    def _():
+        rim_copy.wait_send()
+
+
+def gather_and_project(
+    n_fs, n_sp, x, mix_gain, rope_weight, taps, qd, md, cv, cg, qu, ku, vu, ho, co
+):
+    rows = x.shape[0]
+    bf16, f32 = jnp.bfloat16, jnp.float32
+    vmem = pl.BlockSpec(memory_space=pltpu.VMEM)
+    hbm = pl.BlockSpec(memory_space=pl.ANY)
+
+    def whole(w, dim=0):
+        return (w.shape[0] * n_fs, w.shape[1]) if dim == 0 else (w.shape[0], w.shape[1] * n_fs)
+
+    out_shapes = [
+        ((rows, qd.shape[1]), bf16), ((rows, md.shape[1]), bf16),
+        ((rows, rope_weight.shape[1]), bf16), ((rows, cv.shape[1]), f32),
+        (whole(qu), bf16), (whole(ku), bf16), (whole(vu), bf16),
+        (whole(ho, 1), bf16), (whole(co, 1), bf16),
+    ]
+    dma = pltpu.SemaphoreType.DMA
+    wide = max(qd.shape[1], md.shape[1])
+    return pl.pallas_call(
+        functools.partial(gather_kernel, (n_fs, n_sp)),
+        out_shape=[jax.ShapeDtypeStruct(*o) for o in out_shapes],
+        in_specs=[vmem] * 4 + [hbm] * 9,
+        out_specs=[vmem] * 9,
+        scratch_shapes=[
+            pltpu.VMEM(whole(qd), bf16), pltpu.VMEM(whole(md), bf16),
+            pltpu.VMEM(whole(cv), bf16), pltpu.VMEM(whole(cg), bf16),
+            pltpu.VMEM(x.shape, bf16), pltpu.VMEM((rows, wide), f32),
+            pltpu.VMEM((rows, cv.shape[1]), f32), pltpu.VMEM((rows, cv.shape[1]), f32),
+            pltpu.VMEM((rows + RIM, cv.shape[1]), f32),
+            pltpu.VMEM((RIM, cv.shape[1]), bf16), pltpu.VMEM((RIM, cv.shape[1]), bf16),
+            dma((9, n_fs - 1)), dma((9, n_fs - 1)), dma((9, n_fs - 1)), dma((9, n_fs - 1)),
+            dma((9,)), dma((2,)),
+        ],
+        compiler_params=pltpu.CompilerParams(
+            collective_id=0, has_side_effects=True, vmem_limit_bytes=56 * 1024 * 1024
+        ),
+    )(x, mix_gain[None, :], rope_weight, taps, qd, md, cv, cg, qu, ku, vu, ho, co)
 
 
 def key_block(key_count):
@@ -90,6 +311,14 @@
     while block_size > 2048 and block_size % 2 == 0:
         block_size = block_size // 2
     return block_size
+
+
+def sum_groups(partial):
+    count = lax.axis_size("tp")
+    if count != 2:
+        return lax.psum(partial, "tp")
+    other = lax.ppermute(partial, "tp", [(0, 1), (1, 0)])
+    return (partial.astype(jnp.float32) + other.astype(jnp.float32)).astype(jnp.bfloat16)
 
 
 def local(
@@ -114,37 +343,15 @@
     conv_out,
 ):
     own_rows = tokens[0]
-    normed = norm_rows(own_rows.astype(jnp.float32), mix_gain).astype(jnp.bfloat16)
-    down_query, down_memory, conv_values, conv_gates, up_query, up_keys, up_values = (
-        lax.all_gather(query_down, "fs", axis=0, tiled=True),
-        lax.all_gather(memory_down, "fs", axis=0, tiled=True),
-        lax.all_gather(conv_value, "fs", axis=0, tiled=True),
-        lax.all_gather(conv_gate, "fs", axis=0, tiled=True),
-        lax.all_gather(query_up, "fs", axis=0, tiled=True),
-        lax.all_gather(key_up, "fs", axis=0, tiled=True),
-        lax.all_gather(value_up, "fs", axis=0, tiled=True),
-    )
-    out_heads, out_conv = (
-        lax.all_gather(heads_out, "fs", axis=1, tiled=True),
-        lax.all_gather(conv_out, "fs", axis=1, tiled=True),
-    )
-    joined = jnp.concatenate(
-        [down_query, down_memory, rope_weight, conv_values, conv_gates], axis=1
-    )
-    query_cols = down_query.shape[1]
-    memory_cols = down_memory.shape[1]
-    conv_cols = conv_values.shape[1]
-    projected = jnp.dot(normed, joined, preferred_element_type=jnp.float32)
-    row_count = projected.shape[0]
-    rope_start = query_cols + memory_cols
-    value_start = rope_start + QK_ROPE
-    latent_query = projected[:, :query_cols].astype(jnp.bfloat16)
-    latent_memory = projected[:, query_cols:rope_start].astype(jnp.bfloat16)
-    rope_rows = projected[:, rope_start:value_start].astype(jnp.bfloat16)
-    gated = (
-        projected[:, value_start : value_start + conv_cols]
-        * jax.nn.sigmoid(projected[:, value_start + conv_cols :])
-    ).astype(jnp.bfloat16)
+    (
+        latent_query, latent_memory, rope_rows, conv_sum,
+        up_query, up_keys, up_values, out_heads, out_conv,
+    ) = gather_and_project(
+        lax.axis_size("fs"), lax.axis_size("sp"), own_rows, mix_gain, rope_weight, conv_kernel,
+        query_down, memory_down, conv_value, conv_gate,
+        query_up, key_up, value_up, heads_out, conv_out,
+    )
+    row_count = own_rows.shape[0]
     whole_query, whole_memory = (
         lax.all_gather(latent_query, "tp", axis=1, tiled=True),
         lax.all_gather(latent_memory, "tp", axis=1, tiled=True),
@@ -157,9 +364,6 @@
     head_count = queries.shape[1]
     query_segment = positions // SEG
     score_scale = QK_DIM ** (-0.5)
-    tap_count = conv_kernel.shape[0]
-    left_rim = from_behind(gated[row_count - (tap_count - 1) :], "sp", 1)
-    conv_sum = depthwise(jnp.concatenate([left_rim, gated], axis=0), conv_kernel, row_count)
     row_sums, row_squares = lax.psum(
         (jnp.sum(conv_sum, axis=1), jnp.sum(conv_sum * conv_sum, axis=1)), "tp"
     )
@@ -228,7 +432,7 @@
     mixer_rows = jnp.concatenate([attention, conv_result], axis=1)
     out_weight = jnp.concatenate([out_heads, out_conv], axis=0)
     partial_sum = jnp.dot(mixer_rows, out_weight, preferred_element_type=jnp.float32)
-    mixed = lax.psum(partial_sum.astype(jnp.bfloat16), "tp")
+    mixed = sum_groups(partial_sum.astype(jnp.bfloat16))
     return mixed[None]
 
 

time: 315 us -> 177 us (0.56)
  waiting for transfers between devices: 172 us -> 7.28 us
  Pallas kernels: 0 us -> 110 us
  other arithmetic: 35.9 us -> 8.26 us
  local copies, waits for them, and re-layouts: 27.4 us -> 2.53 us
  blocking collectives: 39.4 us -> 24.4 us
  matrix products: 20.4 us -> 10.1 us
  starting transfers between devices: 3.7 us -> 0.07 us
    all_gather x7 -> x0, waiting for transfers between devices: 147 us -> none  [the longest x1 37.1 us: local(): lax.all_gather(conv_value, 'fs', axis=0, tiled=True)]
    pallas_call x0 -> x1, Pallas kernels: none -> 110 us  [gather_and_project(): pl.pallas_call(functools.partial(gather_kernel, (n_fs, n_sp)), out_shape=...]
    mul x31 -> x0, other arithmetic: 22 us -> none  [add_tap(): return running + window * weight_row]
    psum x1 -> x0, waiting for transfers between devices: 19.6 us -> none  [local(): mixed = lax.psum(partial_sum.astype(jnp.bfloat16), 'tp')]
    all_gather x2 -> x0, blocking collectives: 19.3 us -> none  [the longest x1 10.3 us: local(): lax.all_gather(key_up, 'fs', axis=0, tiled=True)]
    concatenate x1 -> x0, local copies, waits for them, and re-layouts: 12.6 us -> none  [local(): jnp.concatenate([down_query, down_memory, rope_weight, conv_values, conv_...]
    dynamic_slice x62 -> x0, local copies, waits for them, and re-layouts: 8.98 us -> none  [add_tap(): lax.dynamic_slice_in_dim(extended, tap_index, row_count, 0)]
    dot_general x1 -> x0, matrix products: 7.37 us -> none  [local(): projected = jnp.dot(normed, joined, preferred_element_type=jnp.float32)]
  transfers between devices with their start and end apart: 10 -> 2, of which waited for: 6 -> 2; matrix products, arithmetic and copies ran while one was open for 25% -> 2% of each run, Pallas kernels for 0% -> 0%
where the time goes in v1:
time: 177 us; the launch traced here: 176 us
  Pallas kernels  110 us (62%)
  blocking collectives  24.4 us (14%)
  between operations  13.8 us (8%)
  matrix products  10.1 us (6%)
  other arithmetic  8.26 us (5%)
  waiting for transfers between devices  7.28 us (4%)
  local copies, waits for them, and re-layouts  2.53 us (1%)
    pallas_call x1, Pallas kernels, gather_and_project(): pl.pallas_call(functools.partial(gather_kernel, (n_fs, n_sp)), out_shape=...  110 us
    all_gather x1, blocking collectives, local(): rope_piece = lax.all_gather(rope_rows, 'sp', axis=0, tiled=True)  17.1 us
    all_gather x1, waiting for transfers between devices, local(): memory_piece = lax.all_gather(memory_normed, 'sp', axis=0, tiled=True)  4.62 us
  transfers between devices with their start and end apart: 2, of which 2 were waited for; matrix products, arithmetic and copies ran while one was open for 2% of the time, Pallas kernels for 0%

profile of v1, /device:TPU:0, one launch (start us, length us, event | category | flops | bytes accessed | tf_op | source)
XLA Modules:
  0.0 176.3 jit_solution(6272509621163808260)
XLA Ops:
  6.5 0.0 copy-start.5
  6.5 0.0 all-gather.2.cloned.1.call-start
  6.5 1.9 %copy.30.rope_ref = bf16[2048,32]{1,0:T(8,128)(2,1)} copy(bf16[2048,32]{0,1:T(8,128)(2,1)} %param.23) | data formatting | bytes 262144 | tf_op args[4]
  8.5 0.0 copy-start.4
  8.5 109.8 %shard_map.181 = (bf16[256,384]{1,0:T(8,128)(2,1)}, bf16[256,256]{1,0:T(8,128)(2,1)}, bf16[256,32]{1,0:T(8,128)(2,1)}, f32[256,512]{1,0:T(8,128)}, bf16[768,768]...) custom-call(bf16[256,2048]{1,0:T(8,128)(2,1)} %bitcast.45, ...), custom_call_target="tpu_custom_call" | custom-call | tf_op jit(solution)/shard_map/pallas_call | solution.py:288
  118.3 0.0 copy-start.1
  118.3 2.3 %all_gather.12 = bf16[256,512]{1,0:T(8,128)(2,1)S(1)} all-gather(bf16[256,256]{1,0:T(8,128)(2,1)} %get-tuple-element.48), channel_id=1, replica_groups=mesh['sp'=4,'fs'=4,'tp'=2] {'tp'}, dimensions={1}, use_global_device_ids=true | all-gather | bytes 393216 | tf_op jit(solution)/shard_map/all_gather | solution.py:357
  120.6 0.1 fusion.35
  120.8 0.0 copy-start.8
  120.8 0.0 copy-done.5
  120.8 0.8 fusion.37
  121.6 0.0 all-gather.2.cloned.1.call-update
  121.7 1.2 fusion.60
  122.9 17.1 %all_gather.14 = bf16[1024,32]{1,0:T(8,128)(2,1)S(1)} all-gather(bf16[256,32]{1,0:T(8,128)(2,1)} %get-tuple-element.52), channel_id=1, replica_groups=mesh['sp'=4,'fs'=4,'tp'=2] {'sp'}, dimensions={0}, use_global_device_ids=true | all-gather | bytes 81920 | tf_op jit(solution)/shard_map/all_gather | solution.py:403
  140.0 0.1 copy.31
  140.2 2.3 %all_gather.15 = bf16[256,768]{1,0:T(8,128)(2,1)S(1)} all-gather(bf16[256,384]{1,0:T(8,128)(2,1)} %get-tuple-element.53), channel_id=1, replica_groups=mesh['sp'=4,'fs'=4,'tp'=2] {'tp'}, dimensions={1}, use_global_device_ids=true | all-gather | bytes 589824 | tf_op jit(solution)/shard_map/all_gather | solution.py:356
  142.5 0.2 fusion.32
  142.6 0.0 copy-start
  142.6 0.0 copy-start.6
  142.6 0.0 copy-start.7
  142.7 0.0 copy-done.4
  142.7 0.0 copy-done.1
  142.7 0.0 copy-start.3
  142.7 0.6 fusion.41
  143.3 0.1 multiply_reduce_fusion.1
  143.4 0.0 copy-done.8
  143.4 0.1 multiply_multiply_fusion.1
  143.6 2.7 %all-reduce = (f32[256]{0:T(256)S(1)}, f32[256]{0:T(256)S(1)}) all-reduce(f32[256]{0:T(256)S(1)} %get-tuple-element.60, f32[256]{0:T(256)S(1)} %get-tuple-element.59), channel_id=1, replica_groups=mesh['sp'=4,'fs'=4,'tp'=2] {'tp'}, use_global_device_ids=true, to_apply=%region_9.10 | all-reduce | flops 512 | bytes 4096 | tf_op jit(solution)/shard_map/psum | solution.py:367
  146.3 0.1 multiply_cosine_fusion.1
  146.5 0.3 multiply_cosine_fusion
  146.8 0.2 broadcast_compare_fusion
  147.0 0.0 copy-done
  147.0 0.0 copy-done.6
  147.1 0.0 copy-done.7
  147.1 0.3 multiply_convert_fusion
  147.3 4.6 %all-gather.2.cloned.1.call-done = bf16[1024,512]{1,0:T(8,128)(2,1)} async-done(((bf16[256,512]{1,0:T(8,128)(2,1)}), bf16[1024,512]{1,0:T(8,128)(2,1)}) %all-gather.2.cloned.1.call-update) | async-done | bytes 1048592 | tf_op jit(solution)/shard_map/all_gather | solution.py:402
  152.0 0.0 copy-done.3
  152.0 0.0 copy-start.9
  152.0 2.0 %fusion.61 = f32[1024,512]{0,1:T(8,128)S(1)} fusion(bf16[1024,512]{1,0:T(8,128)(2,1)} %all-gather.2.cloned.1.call-done, bf16[512,512]{1,0:T(8,128)(2,1)S(1)} %copy-done.3), kind=kOutput, calls=%fused_computation.94 | convolution fusion | flops 536870912 | bytes 3670016 | tf_op jit(solution)/shard_map/while/body/eval_jaxpr/dot_general | solution.py:65
  154.0 0.1 broadcast_in_dim.87
  154.1 0.4 multiply_reduce_fusion
  154.5 0.0 copy-done.9
  154.5 0.8 multiply_multiply_fusion
  155.3 0.2 slice.52
  155.5 0.1 subtract_convert_fusion
  155.6 1.7 fusion
  157.3 0.0 copy-start.2
  157.3 0.0 copy-start.11
  157.3 2.0 %fusion.1 = f32[256,8]{0,1:T(8,128)S(1)} fusion(f32[8,1024,256]{2,1,0:T(8,128)S(1)} %get-tuple-element.76, f32[256,8]{0,1:T(8,128)S(1)} %broadcast_maximum_fusion, pred[256,1024]{0,1:T(8,128)(4,1)S(1)} %broadcast_compare_fusion), kind=kLoop, calls=%fused_computation.3 | loop fusion | flops 10483712 | bytes 8667136 | tf_op jit(solution)/shard_map/while/body/eval_jaxpr/reduce_sum | solution.py:388
  159.4 0.0 copy-done.2
  159.4 0.0 copy-done.11
  159.4 0.8 convolution_convert_fusion
  160.1 0.0 copy-start.10
  160.2 2.2 %fusion.29 = bf16[256,8,64]{0,2,1:T(8,128)(2,1)S(1)} fusion(bf16[1024,8,64]{0,2,1:T(8,128)(2,1)S(1)} %bitcast.48, f32[8,1024,256]{2,1,0:T(8,128)S(1)} %get-tuple-element.76, f32[256,8]{0,1:T(8,128)S(1)} %broadcast_maximum_fusion, pred[256,1024]{0,1:T(8,128)(4,1)S(1)} %broadcast_compare_fusion, f32[256,8]{0,1:T(8,128)S(1)} %get-tuple-element.68, ...), kind=kOutput, calls=%fused_computation.28 | convolution fusion | flops 279314432 | bytes 9986048 | tf_op jit(solution)/shard_map/while/body/eval_jaxpr/qhk,khd->qhd/dot_general | solution.py:389
  162.4 0.1 copy.34
  162.5 0.0 copy-done.10
  162.5 2.8 %fusion.10 = bf16[256,2048]{1,0:T(8,128)(2,1)S(1)} fusion(bf16[512,2048]{1,0:T(8,128)(2,1)} %get-tuple-element.58, bf16[512,2048]{1,0:T(8,128)(2,1)S(1)} %copy-done.10, bf16[256,512]{1,0:T(8,128)(2,1)S(1)} %multiply_convert_fusion, bf16[256,512]{1,0:T(8,128)(2,1)S(1)} %copy.34), kind=kOutput, calls=%fused_computation.14 | convolution fusion | flops 1083703296 | bytes 5767168 | tf_op jit(solution)/shard_map/dot_general | solution.py:434
  165.4 0.1 collective-permute-start
  165.4 2.6 %collective-permute-done = bf16[256,2048]{1,0:T(8,128)(2,1)S(1)} collective-permute-done((bf16[256,2048]{1,0:T(8,128)(2,1)S(1)}, bf16[256,2048]{1,0:T(8,128)(2,1)S(1)}, u32[]{:S(2)}, u32[]{:S(2)}) %collective-permute-start) | collective-permute-done | bytes 1048608 | tf_op jit(solution)/shard_map/ppermute | solution.py:320
  168.1 1.4 fusion.25
  (14 shorter events, 0.2 us)
Async XLA Ops:
  6.5 114.3 %copy-start.5 = (f32[512]{0:T(512)S(1)}, f32[512]{0:T(512)}, u32[]{:S(2)}) copy-start(f32[512]{0:T(512)} %param.28) | copy-start | bytes 6148
  6.5 145.4 %all-gather.2.cloned.1.call-start = ((), (), s32[]{:S(2)}) async-start(), calls=%async_computation | async-start | bytes 1310720 | tf_op jit(solution)/shard_map/all_gather | solution.py:402
  8.5 134.2 %copy-start.4 = (f32[768]{0:T(1024)S(1)}, f32[768]{0:T(1024)}, u32[]{:S(2)}) copy-start(f32[768]{0:T(1024)} %param.27) | copy-start | bytes 9220
  118.3 24.4 %copy-start.1 = (bf16[768,768]{1,0:T(8,128)(2,1)S(1)}, bf16[768,768]{1,0:T(8,128)(2,1)}, u32[]{:S(2)}) copy-start(bf16[768,768]{1,0:T(8,128)(2,1)} %get-tuple-element.54) | copy-start | bytes 3538948
  120.8 22.7 %copy-start.8 = (f32[96]{0:T(128)S(1)}, f32[96]{0:T(128)}, u32[]{:S(2)}) copy-start(f32[96]{0:T(128)} %param.29) | copy-start | bytes 1156
  142.6 4.4 %copy-start = (f32[256,512]{1,0:T(8,128)S(1)}, f32[256,512]{1,0:T(8,128)}, u32[]{:S(2)}) copy-start(f32[256,512]{1,0:T(8,128)} %get-tuple-element.56) | copy-start | bytes 1572868
  142.6 4.4 %copy-start.6 = (f32[512]{0:T(512)S(1)}, f32[512]{0:T(512)}, u32[]{:S(2)}) copy-start(f32[512]{0:T(512)} %param.35) | copy-start | bytes 6148
  142.6 4.4 %copy-start.7 = (f32[512]{0:T(512)S(1)}, f32[512]{0:T(512)}, u32[]{:S(2)}) copy-start(f32[512]{0:T(512)} %param.34) | copy-start | bytes 6148
  142.7 9.3 %copy-start.3 = (bf16[512,512]{1,0:T(8,128)(2,1)S(1)}, bf16[512,512]{1,0:T(8,128)(2,1)}, u32[]{:S(2)}) copy-start(bf16[512,512]{1,0:T(8,128)(2,1)} %get-tuple-element.50) | copy-start | bytes 1572868
  152.0 2.6 %copy-start.9 = (f32[96]{0:T(128)S(1)}, f32[96]{0:T(128)}, u32[]{:S(2)}) copy-start(f32[96]{0:T(128)} %param.30) | copy-start | bytes 1156
  157.3 2.1 %copy-start.2 = (bf16[1024,512]{1,0:T(8,128)(2,1)S(1)}, bf16[1024,512]{1,0:T(8,128)(2,1)}, u32[]{:S(2)}) copy-start(bf16[1024,512]{1,0:T(8,128)(2,1)} %all-gather.2.cloned.1.call-done) | copy-start | bytes 3145732
  157.3 2.1 %copy-start.11 = (bf16[512,512]{1,0:T(8,128)(2,1)S(1)}, bf16[512,512]{1,0:T(8,128)(2,1)}, u32[]{:S(2)}) copy-start(bf16[512,512]{1,0:T(8,128)(2,1)} %get-tuple-element.55) | copy-start | bytes 1572868
  160.1 2.4 %copy-start.10 = (bf16[512,2048]{1,0:T(8,128)(2,1)S(1)}, bf16[512,2048]{1,0:T(8,128)(2,1)}, u32[]{:S(2)}) copy-start(bf16[512,2048]{1,0:T(8,128)(2,1)} %get-tuple-element.57) | copy-start | bytes 6291460
  165.4 2.7 %collective-permute-start = (bf16[256,2048]{1,0:T(8,128)(2,1)S(1)}, bf16[256,2048]{1,0:T(8,128)(2,1)S(1)}, u32[]{:S(2)}, u32[]{:S(2)}) collective-permute-start(bf16[256,2048]{1,0:T(8,128)(2,1)S(1)} %fusion.10), channel_id=1, source_target_pairs={{0,1},{1,0},{2,3},{3,2},{4,5},{5,4},{6,7},{7,6},{8,9},{9,8},{10,11... | collective-permute-start | bytes 3145736 | tf_op jit(solution)/shard_map/ppermute | solution.py:320
Sparse Core Ops, SparseCore 0:
  121.8 30.1 all-gather.1

commit v2 on v1

--- a/solution.py
+++ b/solution.py
@@ -82,36 +82,35 @@
 
 def gather_kernel(
     sizes,
-    x_ref, gain_ref, rope_ref, taps_ref,
+    x_ref, gain_ref, rope_ref, taps_ref, cgain_ref, cshift_ref,
     qd, md, cv, cg, qu, ku, vu, ho, co,
-    lq_ref, lm_ref, rr_ref, sum_ref, qu_all, ku_all, vu_all, ho_all, co_all,
-    qd_all, md_all, cv_all, cg_all, normed, acc_q, acc_v, acc_g, ext, tail, rim,
-    send_a, recv_a, send_z, recv_z, local_sem, rim_sem,
+    lq_all, lm_all, rr_all, conv_ref, qu_all, ku_all, vu_all, ho_all, co_all,
+    qd_all, md_all, cv_all, cg_all, normed, acc_q, acc_m, acc_v, acc_g, ext, tail, rim,
+    sums, stats, stats_all,
+    send_d, recv_d, send_r, recv_r, send_z, recv_z, local_sem, rim_sem,
+    sp_send, sp_recv, rr_send, rr_recv, tp_send, tp_recv,
 ):
-    n_fs, n_sp = sizes
+    n_fs, n_sp, n_tp = sizes
     paired = n_sp % 2 == 0
     f = lax.axis_index("fs")
     s = lax.axis_index("sp")
+    t = lax.axis_index("tp")
     parity = lax.rem(s, 2)
     partner = s + 1 - 2 * parity
 
     barrier = pltpu.get_barrier_semaphore()
-    for k in range(1, n_fs):
-        pl.semaphore_signal(
-            barrier, inc=1, device_id={"fs": lax.rem(f + k, n_fs)}, device_id_type=MESH_ID
-        )
-
-    beside = sorted({1 % n_sp, (n_sp - 1) % n_sp} - {0})
-    for step in beside:
-        pl.semaphore_signal(
-            barrier, inc=1, device_id={"sp": lax.rem(s + step, n_sp)}, device_id_type=MESH_ID
-        )
-    pl.semaphore_wait(barrier, n_fs - 1 + len(beside))
+    for axis, at, count in (("fs", f, n_fs), ("sp", s, n_sp), ("tp", t, n_tp)):
+        for k in range(1, count):
+            pl.semaphore_signal(
+                barrier, inc=1, device_id={axis: lax.rem(at + k, count)}, device_id_type=MESH_ID
+            )
+    pl.semaphore_wait(barrier, n_fs + n_sp + n_tp - 3)
 
     jobs = [
         (qd, qd_all, 0), (md, md_all, 0), (cv, cv_all, 0), (cg, cg_all, 0),
         (qu, qu_all, 0), (ku, ku_all, 0), (vu, vu_all, 0), (ho, ho_all, 1), (co, co_all, 1),
     ]
+    last = len(jobs) - 1
 
     def place(whole, shard, dim, owner, start, count):
         rows, cols = shard.shape
@@ -122,38 +121,90 @@
             pl.ds(pl.multiple_of(owner * cols, 128), cols),
         ]
 
-    first, relay, own = [], [], []
+    square = n_fs == 4
+    if square:
+        near_x = f + 1 - 2 * lax.rem(f, 2)
+        near_y = lax.rem(f + 2, 4)
+        far = lax.rem(near_x + 2, 4)
+        targets = sources = [near_x, near_y]
+    else:
+        targets = [lax.rem(f + k, n_fs) for k in range(1, n_fs)]
+        sources = [lax.rem(f + n_fs - k, n_fs) for k in range(1, n_fs)]
+
+    direct, far_copies, over_sp, own = [], [], [], []
     for a, (shard, whole, dim) in enumerate(jobs):
         rows = shard.shape[0]
-        less = relayed_rows(rows, paired)
+        less = 0 if a == last else relayed_rows(rows, paired)
         start = parity * less
-        for k in range(1, n_fs):
-            copy = pltpu.make_async_remote_copy(
-                src_ref=shard.at[pl.ds(pl.multiple_of(start, 16), rows - less), :],
-                dst_ref=place(whole, shard, dim, f, start, rows - less),
-                send_sem=send_a.at[a, k - 1],
-                recv_sem=recv_a.at[a, k - 1],
-                device_id={"fs": lax.rem(f + k, n_fs)},
-                device_id_type=MESH_ID,
+        count = rows - less
+        direct.append([
+            pltpu.make_async_remote_copy(
+                src_ref=shard.at[pl.ds(pl.multiple_of(start, 16), count), :],
+                dst_ref=place(whole, shard, dim, f, start, count),
+                send_sem=send_d.at[a, k], recv_sem=recv_d.at[a, k],
+                device_id={"fs": target}, device_id_type=MESH_ID,
             )
+            for k, target in enumerate(targets)
+        ])
+        halves = []
+        if square:
+            half = (count // 2 + 15) // 16 * 16
+            for k, (owner, target, begin, size) in enumerate((
+                (near_y, near_x, start, half), (near_x, near_y, start + half, count - half)
+            )):
+                piece = place(whole, shard, dim, owner, begin, size)
+                halves.append(pltpu.make_async_remote_copy(
+                    src_ref=piece, dst_ref=piece,
+                    send_sem=send_r.at[a, k], recv_sem=recv_r.at[a, k],
+                    device_id={"fs": target}, device_id_type=MESH_ID,
+                ))
+        far_copies.append(halves)
+        across = []
+        if less:
+            lack = parity * (rows - less)
+            for k, owner in enumerate(sources + ([far] if square else [])):
+                piece = place(whole, shard, dim, owner, lack, less)
+                across.append(pltpu.make_async_remote_copy(
+                    src_ref=piece, dst_ref=piece,
+                    send_sem=send_z.at[a, k], recv_sem=recv_z.at[a, k],
+                    device_id={"sp": partner}, device_id_type=MESH_ID,
+                ))
+        over_sp.append(across)
+        own.append(pltpu.make_async_copy(
+            shard, place(whole, shard, dim, f, 0, rows), local_sem.at[a]
+        ))
+
+    def begin_array(a):
+        if a <= last:
+            for copy in direct[a]:
+                copy.start()
+
+    def finish_far(a):
+        for copy in far_copies[a]:
+            copy.wait_recv()
+        for copy in over_sp[a][len(sources):]:
             copy.start()
-            first.append(copy)
-            if less:
-                lack = parity * (rows - less)
-                owner = lax.rem(f + n_fs - k, n_fs)
-                relay.append(pltpu.make_async_remote_copy(
-                    src_ref=place(whole, shard, dim, owner, lack, less),
-                    dst_ref=place(whole, shard, dim, owner, lack, less),
-                    send_sem=send_z.at[a, k - 1],
-                    recv_sem=recv_z.at[a, k - 1],
-                    device_id={"sp": partner},
-                    device_id_type=MESH_ID,
-                ))
-        mine = pltpu.make_async_copy(
-            shard, place(whole, shard, dim, f, 0, rows), local_sem.at[a]
-        )
-        mine.start()
-        own.append(mine)
+
+    def tick(a):
+        for copy in direct[a]:
+            copy.wait_recv()
+        for copy in far_copies[a]:
+            copy.start()
+        begin_array(a + 3)
+        for copy in over_sp[a][: len(sources)]:
+            copy.start()
+        if a >= 1:
+            finish_far(a - 1)
+
+    def complete(a):
+        own[a].wait()
+        for copy in over_sp[a]:
+            copy.wait_recv()
+
+    for a in range(3):
+        begin_array(a)
+    for copy in own:
+        copy.start()
 
     rows = x_ref.shape[0]
     part = 32
@@ -165,20 +216,6 @@
         scale = lax.rsqrt(jnp.mean(x * x, axis=-1, keepdims=True) + epsilon)
         normed[at, :] = (x * scale * gain_ref[...]).astype(jnp.bfloat16)
 
-    per = n_fs - 1
-
-    def pass_on(a):
-        for k in range(per):
-            first[a * per + k].wait_recv()
-            if paired:
-                relay[a * per + k].start()
-
-    def complete(a):
-        own[a].wait()
-        if paired:
-            for k in range(per):
-                relay[a * per + k].wait_recv()
-
     depth = qd.shape[0]
 
     def project(weight, acc):
@@ -191,26 +228,57 @@
                 normed[:, at], weight[at, :], preferred_element_type=jnp.float32
             )
 
-    rr_ref[...] = jnp.dot(
+    mine = pl.ds(pl.multiple_of(s * rows, 16), rows)
+    rr_all[mine, :] = jnp.dot(
         normed[...], rope_ref[...], preferred_element_type=jnp.float32
     ).astype(jnp.bfloat16)
-    pass_on(0)
-    pass_on(1)
+    tick(0)
+    tick(1)
+    tick(2)
     complete(0)
     project(qd_all, acc_q)
-    lq_ref[...] = acc_q[...].astype(jnp.bfloat16)
-    pass_on(2)
+    lq_all[t, :, :] = acc_q[...].astype(jnp.bfloat16)
+    tick(3)
     complete(1)
-    acc_m = acc_q.at[:, pl.ds(0, md.shape[1])]
     project(md_all, acc_m)
-    lm_ref[...] = acc_m[...].astype(jnp.bfloat16)
-    pass_on(3)
+    lm_all[t, mine, :] = acc_m[...].astype(jnp.bfloat16)
+    tick(4)
     complete(2)
     project(cv_all, acc_v)
-    pass_on(4)
+
+    exchanges, passes = [], []
+    for k in range(1, n_sp):
+        peer = {"sp": lax.rem(s + k, n_sp)}
+        exchanges.append(pltpu.make_async_remote_copy(
+            src_ref=lm_all.at[t, mine, :], dst_ref=lm_all.at[t, mine, :],
+            send_sem=sp_send.at[k - 1], recv_sem=sp_recv.at[k - 1],
+            device_id=peer, device_id_type=MESH_ID,
+        ))
+        exchanges.append(pltpu.make_async_remote_copy(
+            src_ref=rr_all.at[mine, :], dst_ref=rr_all.at[mine, :],
+            send_sem=rr_send.at[k - 1], recv_sem=rr_recv.at[k - 1],
+            device_id=peer, device_id_type=MESH_ID,
+        ))
+    tp_peers = [{"tp": lax.rem(t + k, n_tp)} for k in range(1, n_tp)]
+
+    def to_tp(kind, source, landing):
+        return [
+            pltpu.make_async_remote_copy(
+                src_ref=source, dst_ref=landing(k),
+                send_sem=tp_send.at[kind, k], recv_sem=tp_recv.at[kind, k],
+                device_id=peer, device_id_type=MESH_ID,
+            )
+            for k, peer in enumerate(tp_peers)
+        ]
+
+    query_copies = to_tp(0, lq_all.at[t], lambda k: lq_all.at[t])
+    memory_copies = to_tp(1, lm_all.at[t], lambda k: lm_all.at[t])
+    stat_copies = to_tp(2, stats, lambda k: stats_all.at[k])
+    for copy in exchanges + query_copies:
+        copy.start()
+    tick(5)
     complete(3)
     project(cg_all, acc_g)
-    pass_on(5)
 
     @pl.loop(0, rows // part)
     def _(i):
@@ -223,12 +291,16 @@
         src_ref=tail, dst_ref=rim, send_sem=rim_sem.at[0], recv_sem=rim_sem.at[1],
         device_id={"sp": lax.rem(s + 1, n_sp)}, device_id_type=MESH_ID,
     )
+    tick(6)
 
     @pl.when(s < n_sp - 1)
     def _():
         rim_copy.start()
 
-    pass_on(6)
+    for copy in exchanges:
+        copy.wait_recv()
+    for copy in memory_copies:
+        copy.start()
 
     @pl.when(s > 0)
     def _():
@@ -239,7 +311,6 @@
     def _():
         ext[pl.ds(0, RIM), :] = jnp.zeros((RIM, ext.shape[1]), jnp.float32)
 
-    pass_on(7)
     tap_count = taps_ref.shape[0]
     block = 64
 
@@ -253,12 +324,53 @@
                 total = total + ext[
                     pl.ds(r + RIM - (tap_count - 1) + j, block), cols
                 ] * taps[j : j + 1, :]
-            sum_ref[pl.ds(r, block), cols] = total
-
-    pass_on(8)
-    for a in range(4, 9):
+            sums[pl.ds(r, block), cols] = total
+
+    @pl.loop(0, rows // part)
+    def _(i):
+        begin = pl.multiple_of(i * part, part)
+        values = sums[pl.ds(begin, part), :]
+        stats[pl.ds(begin, part), :] = jnp.broadcast_to(
+            jnp.sum(values, axis=1, keepdims=True), (part, 128)
+        )
+        stats[pl.ds(pl.multiple_of(rows + begin, part), part), :] = jnp.broadcast_to(
+            jnp.sum(values * values, axis=1, keepdims=True), (part, 128)
+        )
+
+    tick(7)
+    for copy in stat_copies:
+        copy.start()
+    tick(8)
+    for copy in stat_copies:
+        copy.wait_recv()
+
+    channels = ext.shape[1] * n_tp
+
+    @pl.loop(0, rows // part)
+    def _(i):
+        begin = pl.multiple_of(i * part, part)
+        upper = pl.ds(begin, part)
+        lower = pl.ds(pl.multiple_of(rows + begin, part), part)
+        total, squares = stats[upper, :], stats[lower, :]
+        for k in range(n_tp - 1):
+            total = total + stats_all[k, upper, :]
+            squares = squares + stats_all[k, lower, :]
+        mean = total[:, :1] / channels
+        spread = squares[:, :1] / channels - mean * mean
+        shaped = (sums[upper, :] - mean) * lax.rsqrt(spread + epsilon)
+        conv_ref[upper, :] = jax.nn.silu(
+            shaped * cgain_ref[...] + cshift_ref[...]
+        ).astype(jnp.bfloat16)
+
+    finish_far(last)
+    for a in range(4, last + 1):
         complete(a)
-    for copy in first + relay:
+    for copy in query_copies + memory_copies:
+        copy.wait_recv()
+    for group in direct + far_copies + over_sp:
+        for copy in group:
+            copy.wait_send()
+    for copy in exchanges + query_copies + memory_copies + stat_copies:
         copy.wait_send()
 
     @pl.when(s < n_sp - 1)
@@ -267,8 +379,10 @@
 
 
 def gather_and_project(
-    n_fs, n_sp, x, mix_gain, rope_weight, taps, qd, md, cv, cg, qu, ku, vu, ho, co
+    sizes, x, mix_gain, rope_weight, taps, channel_gain, channel_shift,
+    qd, md, cv, cg, qu, ku, vu, ho, co,
 ):
+    n_fs, n_sp, n_tp = sizes
     rows = x.shape[0]
     bf16, f32 = jnp.bfloat16, jnp.float32
     vmem = pl.BlockSpec(memory_space=pltpu.VMEM)
@@ -278,32 +392,41 @@
         return (w.shape[0] * n_fs, w.shape[1]) if dim == 0 else (w.shape[0], w.shape[1] * n_fs)
 
     out_shapes = [
-        ((rows, qd.shape[1]), bf16), ((rows, md.shape[1]), bf16),
-        ((rows, rope_weight.shape[1]), bf16), ((rows, cv.shape[1]), f32),
+        ((n_tp, rows, qd.shape[1]), bf16), ((n_tp, n_sp * rows, md.shape[1]), bf16),
+        ((n_sp * rows, rope_weight.shape[1]), bf16), ((rows, cv.shape[1]), bf16),
         (whole(qu), bf16), (whole(ku), bf16), (whole(vu), bf16),
         (whole(ho, 1), bf16), (whole(co, 1), bf16),
     ]
     dma = pltpu.SemaphoreType.DMA
-    wide = max(qd.shape[1], md.shape[1])
+    tp_others = max(n_tp - 1, 1)
+    sp_others = max(n_sp - 1, 1)
     return pl.pallas_call(
-        functools.partial(gather_kernel, (n_fs, n_sp)),
+        functools.partial(gather_kernel, sizes),
         out_shape=[jax.ShapeDtypeStruct(*o) for o in out_shapes],
-        in_specs=[vmem] * 4 + [hbm] * 9,
+        in_specs=[vmem] * 6 + [hbm] * 9,
         out_specs=[vmem] * 9,
         scratch_shapes=[
             pltpu.VMEM(whole(qd), bf16), pltpu.VMEM(whole(md), bf16),
             pltpu.VMEM(whole(cv), bf16), pltpu.VMEM(whole(cg), bf16),
-            pltpu.VMEM(x.shape, bf16), pltpu.VMEM((rows, wide), f32),
+            pltpu.VMEM(x.shape, bf16), pltpu.VMEM((rows, qd.shape[1]), f32),
+            pltpu.VMEM((rows, md.shape[1]), f32),
             pltpu.VMEM((rows, cv.shape[1]), f32), pltpu.VMEM((rows, cv.shape[1]), f32),
             pltpu.VMEM((rows + RIM, cv.shape[1]), f32),
             pltpu.VMEM((RIM, cv.shape[1]), bf16), pltpu.VMEM((RIM, cv.shape[1]), bf16),
-            dma((9, n_fs - 1)), dma((9, n_fs - 1)), dma((9, n_fs - 1)), dma((9, n_fs - 1)),
-            dma((9,)), dma((2,)),
+            pltpu.VMEM((rows, cv.shape[1]), f32), pltpu.VMEM((2 * rows, 128), f32),
+            pltpu.VMEM((tp_others, 2 * rows, 128), f32),
+            dma((9, n_fs - 1)), dma((9, n_fs - 1)), dma((9, 2)), dma((9, 2)),
+            dma((9, n_fs - 1)), dma((9, n_fs - 1)), dma((9,)), dma((2,)),
+            dma((sp_others,)), dma((sp_others,)), dma((sp_others,)), dma((sp_others,)),
+            dma((3, tp_others)), dma((3, tp_others)),
         ],
         compiler_params=pltpu.CompilerParams(
             collective_id=0, has_side_effects=True, vmem_limit_bytes=56 * 1024 * 1024
         ),
-    )(x, mix_gain[None, :], rope_weight, taps, qd, md, cv, cg, qu, ku, vu, ho, co)
+    )(
+        x, mix_gain[None, :], rope_weight, taps, channel_gain[None, :], channel_shift[None, :],
+        qd, md, cv, cg, qu, ku, vu, ho, co,
+    )
 
 
 def key_block(key_count):
@@ -344,36 +467,25 @@
 ):
     own_rows = tokens[0]
     (
-        latent_query, latent_memory, rope_rows, conv_sum,
+        query_parts, memory_parts, rope_piece, conv_result,
         up_query, up_keys, up_values, out_heads, out_conv,
     ) = gather_and_project(
-        lax.axis_size("fs"), lax.axis_size("sp"), own_rows, mix_gain, rope_weight, conv_kernel,
+        (lax.axis_size("fs"), lax.axis_size("sp"), lax.axis_size("tp")),
+        own_rows, mix_gain, rope_weight, conv_kernel, channel_gain, channel_shift,
         query_down, memory_down, conv_value, conv_gate,
         query_up, key_up, value_up, heads_out, conv_out,
     )
     row_count = own_rows.shape[0]
-    whole_query, whole_memory = (
-        lax.all_gather(latent_query, "tp", axis=1, tiled=True),
-        lax.all_gather(latent_memory, "tp", axis=1, tiled=True),
-    )
+    whole_query = jnp.concatenate(list(query_parts), axis=1)
+    whole_memory = jnp.concatenate(list(memory_parts), axis=1)
     query_normed = norm_rows(whole_query.astype(jnp.float32), latent_gain).astype(jnp.bfloat16)
-    memory_normed = norm_rows(whole_memory.astype(jnp.float32), memory_gain).astype(jnp.bfloat16)
+    memory_piece = norm_rows(whole_memory.astype(jnp.float32), memory_gain).astype(jnp.bfloat16)
     positions = lax.axis_index("sp") * row_count + jnp.arange(row_count, dtype=jnp.int32)
     cosine_table, sine_table = rope_tables(positions)
     queries = heads_query(query_normed, up_query, query_gain, cosine_table, sine_table)
     head_count = queries.shape[1]
     query_segment = positions // SEG
     score_scale = QK_DIM ** (-0.5)
-    row_sums, row_squares = lax.psum(
-        (jnp.sum(conv_sum, axis=1), jnp.sum(conv_sum * conv_sum, axis=1)), "tp"
-    )
-    row_mean = row_sums / CONV_W
-    spread = row_squares / CONV_W - row_mean * row_mean
-    centered = conv_sum - row_mean[:, None]
-    conv_result = jax.nn.silu(
-        centered * lax.rsqrt(spread[:, None] + epsilon) * channel_gain + channel_shift
-    ).astype(jnp.bfloat16)
-
     def attend(state_carry, key_rows, value_rows, key_pos):
         running_max, row_total, weighted = state_carry
         scores = (
@@ -399,9 +511,6 @@
         jnp.zeros((row_count, head_count), jnp.float32),
         jnp.zeros((row_count, head_count, V_DIM), jnp.float32),
     )
-    memory_piece = lax.all_gather(memory_normed, "sp", axis=0, tiled=True)
-    rope_piece = lax.all_gather(rope_rows, "sp", axis=0, tiled=True)
-
     def block_keys(block_start, block_size):
         memory_block = lax.dynamic_slice_in_dim(memory_piece, block_start, block_size, 0)
         rope_block = lax.dynamic_slice_in_dim(rope_piece, block_start, block_size, 0)

time: 177 us -> 127 us (0.72)
  blocking collectives: 24.4 us -> 0 us
  between operations: 13.8 us -> 0.4 us
  Pallas kernels: 110 us -> 105 us
  waiting for transfers between devices: 7.28 us -> 2.65 us
  other arithmetic: 8.26 us -> 6.13 us
    all_gather x3 -> x0, blocking collectives: 21.8 us -> none  [the longest x1 17.1 us: local(): rope_piece = lax.all_gather(rope_rows, 'sp', axis=0, tiled=True)]
    pallas_call x1, Pallas kernels: 110 us -> 105 us  [gather_and_project(): pl.pallas_call(functools.partial(gather_kernel, sizes), out_shape=[jax.Sh...]
    all_gather x1 -> x0, waiting for transfers between devices: 4.62 us -> none  [local(): memory_piece = lax.all_gather(memory_normed, 'sp', axis=0, tiled=True)]
    psum x1 -> x0, blocking collectives: 2.65 us -> none  [local(): lax.psum((jnp.sum(conv_sum, axis=1), jnp.sum(conv_sum * conv_sum, axis=1)...]
  transfers between devices with their start and end apart: 2 -> 1, of which waited for: 2 -> 1; matrix products, arithmetic and copies ran while one was open for 2% -> 0% of each run, Pallas kernels for 0% -> 0%
where the time goes in v2:
time: 127 us
  Pallas kernels  105 us (83%)
  matrix products  9.17 us (7%)
  other arithmetic  6.13 us (5%)
  local copies, waits for them, and re-layouts  4.04 us (3%)
  waiting for transfers between devices  2.65 us (2%)
    pallas_call x1, Pallas kernels, gather_and_project(): pl.pallas_call(functools.partial(gather_kernel, sizes), out_shape=[jax.Sh...  105 us
    dot_general x1, matrix products, local(): jnp.dot(mixer_rows, out_weight, preferred_element_type=jnp.float32)  2.84 us
    ppermute x1, waiting for transfers between devices, sum_groups(): other = lax.ppermute(partial, 'tp', [(0, 1), (1, 0)])  2.65 us
  transfers between devices with their start and end apart: 1, of which 1 were waited for; matrix products, arithmetic and copies ran while one was open for 0% of the time, Pallas kernels for 0%

profile of v2, /device:TPU:0, one launch (start us, length us, event | category | flops | bytes accessed | tf_op | source)
XLA Modules:
  0.0 127.1 jit_solution(15492899195943882402)
XLA Ops:
  0.0 0.1 multiply_cosine_fusion.1
  0.2 0.3 multiply_cosine_fusion
  0.5 1.9 %copy.25.rope_ref = bf16[2048,32]{1,0:T(8,128)(2,1)} copy(bf16[2048,32]{0,1:T(8,128)(2,1)} %param.23) | data formatting | bytes 262144 | tf_op args[4]
  2.4 104.6 %shard_map.181 = (bf16[2,256,384]{2,1,0:T(8,128)(2,1)}, bf16[2,1024,256]{2,1,0:T(8,128)(2,1)}, bf16[1024,32]{1,0:T(8,128)(2,1)}, bf16[256,512]{1,0:T(8,128)(2,1)...) custom-call(bf16[256,2048]{1,0:T(8,128)(2,1)} %bitcast.53, ...), custom_call_target="tpu_custom_call" | custom-call | tf_op jit(solution)/shard_map/pallas_call | solution.py:403
  107.0 0.0 copy-start.1
  107.1 0.0 copy-start
  107.1 0.0 copy-start.5
  107.1 0.0 copy-start.9
  107.1 1.4 %slice_bitcast_fusion.1 = (bf16[1024,256]{1,0:T(8,128)(2,1)S(1)}, bf16[1024,256]{1,0:T(8,128)(2,1)S(1)}) fusion(bf16[2,1024,256]{2,1,0:T(8,128)(2,1)} %get-tuple-element.48), kind=kLoop, calls=%fused_computation.49 | loop fusion | bytes 2097152 | tf_op jit(solution)/shard_map/unstack | solution.py:480
  108.5 0.0 copy-start.2
  108.5 0.3 fusion.13
  108.8 0.0 copy-done.1
  108.8 0.1 copy.26
  108.9 0.0 copy-done
  108.9 0.0 copy-start.7
  108.9 0.0 copy-start.10
  109.0 0.2 fusion.35
  109.2 0.0 copy-done.5
  109.2 0.0 copy-done.9
  109.2 0.6 fusion.41
  109.8 0.1 multiply_reduce_fusion.1
  109.9 0.0 copy-done.2
  109.9 0.0 copy-start.6
  109.9 0.1 multiply_multiply_fusion.1
  110.1 0.0 copy-done.7
  110.1 0.0 copy-done.10
  110.2 0.9 convolution_convert_fusion
  111.1 0.0 copy-done.6
  111.1 0.9 fusion.62
  112.0 0.0 copy-start.3
  112.0 0.1 broadcast_in_dim.91
  112.1 0.4 multiply_reduce_fusion
  112.6 0.1 copy-done.3
  112.7 0.6 multiply_multiply_fusion
  113.3 0.2 slice.52
  113.4 0.2 broadcast_compare_fusion
  113.7 0.1 subtract_convert_fusion
  113.8 1.7 %fusion = (f32[256,8]{0,1:T(8,128)S(1)}, f32[8,1024,256]{2,1,0:T(8,128)S(1)}) fusion(pred[256,1024]{0,1:T(8,128)(4,1)S(1)} %broadcast_compare_fusion, bf16[256,8,16]{0,2,1:T(8,128)(2,1)S(1)} %get-tuple-element.64, bf16[256,8,16]{0,2,1:T(8,128)(2,1)S(1)} %get-tuple-element.63, bf16[256,8,64]{0,2,1:T(8,128)(2,1)S(1)} %slice.53, ...), kind=kOutput, calls=%fused_computation.2 | convolution fusion | flops 414840832 | bytes 10625024 | tf_op jit(solution)/shard_map/while/body/eval_jaxpr/qhd,khd->qhk/dot_general | solution.py:492
  115.5 2.2 %fusion.1 = f32[256,8]{0,1:T(8,128)S(1)} fusion(f32[8,1024,256]{2,1,0:T(8,128)S(1)} %get-tuple-element.74, f32[256,8]{0,1:T(8,128)S(1)} %broadcast_maximum_fusion, pred[256,1024]{0,1:T(8,128)(4,1)S(1)} %broadcast_compare_fusion), kind=kLoop, calls=%fused_computation.3 | loop fusion | flops 10483712 | bytes 8667136 | tf_op jit(solution)/shard_map/while/body/eval_jaxpr/reduce_sum | solution.py:500
  117.7 0.0 copy-start.4
  117.8 0.0 copy-start.8
  117.8 2.2 %fusion.32 = bf16[256,8,64]{0,2,1:T(8,128)(2,1)S(1)} fusion(bf16[1024,8,64]{0,2,1:T(8,128)(2,1)S(1)} %bitcast.58, f32[8,1024,256]{2,1,0:T(8,128)S(1)} %get-tuple-element.74, f32[256,8]{0,1:T(8,128)S(1)} %broadcast_maximum_fusion, pred[256,1024]{0,1:T(8,128)(4,1)S(1)} %broadcast_compare_fusion, f32[256,8]{0,1:T(8,128)S(1)} %get-tuple-element.68, ...), kind=kOutput, calls=%fused_computation.34 | convolution fusion | flops 279314432 | bytes 9986048 | tf_op jit(solution)/shard_map/while/body/eval_jaxpr/qhk,khd->qhd/dot_general | solution.py:501
  120.0 0.1 copy.29
  120.1 0.0 copy-done.4
  120.1 0.0 copy-done.8
  120.1 2.8 %fusion.10 = bf16[256,2048]{1,0:T(8,128)(2,1)S(1)} fusion(bf16[512,2048]{1,0:T(8,128)(2,1)} %get-tuple-element.58, bf16[512,2048]{1,0:T(8,128)(2,1)S(1)} %copy-done.4, bf16[256,512]{1,0:T(8,128)(2,1)S(1)} %copy-done.8, bf16[256,512]{1,0:T(8,128)(2,1)S(1)} %copy.29), kind=kOutput, calls=%fused_computation.16 | convolution fusion | flops 1083703296 | bytes 5767168 | tf_op jit(solution)/shard_map/dot_general | solution.py:543
  123.0 0.1 collective-permute-start
  123.1 2.6 %collective-permute-done = bf16[256,2048]{1,0:T(8,128)(2,1)S(1)} collective-permute-done((bf16[256,2048]{1,0:T(8,128)(2,1)S(1)}, bf16[256,2048]{1,0:T(8,128)(2,1)S(1)}, u32[]{:S(2)}, u32[]{:S(2)}) %collective-permute-start) | collective-permute-done | bytes 1048608 | tf_op jit(solution)/shard_map/ppermute | solution.py:443
  125.7 1.4 %fusion.28 = bf16[1,256,2048]{2,1,0:T(8,128)(2,1)} fusion(bf16[256,2048]{1,0:T(8,128)(2,1)S(1)} %collective-permute-done, bf16[256,2048]{1,0:T(8,128)(2,1)S(1)} %fusion.10), kind=kLoop, calls=%fused_computation.31 | loop fusion | flops 2097152 | bytes 3145728 | tf_op jit(solution)/shard_map/broadcast_in_dim | solution.py:545
  (13 shorter events, 0.2 us)
Async XLA Ops:
  107.0 1.7 %copy-start.1 = (bf16[1024,32]{1,0:T(8,128)(2,1)S(1)}, bf16[1024,32]{1,0:T(8,128)(2,1)}, u32[]{:S(2)}) copy-start(bf16[1024,32]{1,0:T(8,128)(2,1)} %get-tuple-element.52) | copy-start | bytes 196612
  107.1 1.9 %copy-start = (bf16[2,256,384]{2,1,0:T(8,128)(2,1)S(1)}, bf16[2,256,384]{2,1,0:T(8,128)(2,1)}, u32[]{:S(2)}) copy-start(bf16[2,256,384]{2,1,0:T(8,128)(2,1)} %get-tuple-element.53) | copy-start | bytes 1179652
  107.1 2.1 %copy-start.5 = (bf16[768,768]{1,0:T(8,128)(2,1)S(1)}, bf16[768,768]{1,0:T(8,128)(2,1)}, u32[]{:S(2)}) copy-start(bf16[768,768]{1,0:T(8,128)(2,1)} %get-tuple-element.54) | copy-start | bytes 3538948
  107.1 2.1 %copy-start.9 = (f32[768]{0:T(1024)S(1)}, f32[768]{0:T(1024)}, u32[]{:S(2)}) copy-start(f32[768]{0:T(1024)} %param.27) | copy-start | bytes 9220
  108.5 1.4 %copy-start.2 = (f32[96]{0:T(128)S(1)}, f32[96]{0:T(128)}, u32[]{:S(2)}) copy-start(f32[96]{0:T(128)} %param.29) | copy-start | bytes 1156
  108.9 1.2 copy-start.7
  108.9 1.2 copy-start.10
  109.9 1.1 copy-start.6
  112.0 0.7 copy-start.3
  117.7 2.4 %copy-start.4 = (bf16[512,2048]{1,0:T(8,128)(2,1)S(1)}, bf16[512,2048]{1,0:T(8,128)(2,1)}, u32[]{:S(2)}) copy-start(bf16[512,2048]{1,0:T(8,128)(2,1)} %get-tuple-element.57) | copy-start | bytes 6291460
  117.8 2.4 %copy-start.8 = (bf16[256,512]{1,0:T(8,128)(2,1)S(1)}, bf16[256,512]{1,0:T(8,128)(2,1)}, u32[]{:S(2)}) copy-start(bf16[256,512]{1,0:T(8,128)(2,1)} %get-tuple-element.56) | copy-start | bytes 786436
  123.0 2.7 %collective-permute-start = (bf16[256,2048]{1,0:T(8,128)(2,1)S(1)}, bf16[256,2048]{1,0:T(8,128)(2,1)S(1)}, u32[]{:S(2)}, u32[]{:S(2)}) collective-permute-start(bf16[256,2048]{1,0:T(8,128)(2,1)S(1)} %fusion.10), channel_id=1, source_target_pairs={{0,1},{1,0},{2,3},{3,2},{4,5},{5,4},{6,7},{7,6},{8,9},{9,8},{10,11... | collective-permute-start | bytes 3145736 | tf_op jit(solution)/shard_map/ppermute | solution.py:443

commit v3 on v2

--- a/solution.py
+++ b/solution.py
@@ -77,7 +77,7 @@
 
 
 def relayed_rows(rows, paired):
-    return (rows * 3 // 8) // 16 * 16 if paired else 0
+    return (rows * 5 // 16) // 16 * 16 if paired else 0
 
 
 def gather_kernel(
@@ -111,6 +111,7 @@
         (qu, qu_all, 0), (ku, ku_all, 0), (vu, vu_all, 0), (ho, ho_all, 1), (co, co_all, 1),
     ]
     last = len(jobs) - 1
+    ahead = 4
 
     def place(whole, shard, dim, owner, start, count):
         rows, cols = shard.shape
@@ -190,7 +191,7 @@
             copy.wait_recv()
         for copy in far_copies[a]:
             copy.start()
-        begin_array(a + 3)
+        begin_array(a + ahead)
         for copy in over_sp[a][: len(sources)]:
             copy.start()
         if a >= 1:
@@ -201,7 +202,7 @@
         for copy in over_sp[a]:
             copy.wait_recv()
 
-    for a in range(3):
+    for a in range(ahead):
         begin_array(a)
     for copy in own:
         copy.start()
@@ -314,8 +315,7 @@
     tap_count = taps_ref.shape[0]
     block = 64
 
-    @pl.loop(0, ext.shape[1] // 128)
-    def _(c):
+    def convolve(c):
         cols = pl.ds(pl.multiple_of(c * 128, 128), 128)
         taps = taps_ref[:, cols].astype(jnp.float32)
         for r in range(0, rows, block):
@@ -325,6 +325,11 @@
                     pl.ds(r + RIM - (tap_count - 1) + j, block), cols
                 ] * taps[j : j + 1, :]
             sums[pl.ds(r, block), cols] = total
+
+    tiles = ext.shape[1] // 128
+    pl.loop(0, tiles // 2)(convolve)
+    tick(7)
+    pl.loop(tiles // 2, tiles)(convolve)
 
     @pl.loop(0, rows // part)
     def _(i):
@@ -337,10 +342,9 @@
             jnp.sum(values * values, axis=1, keepdims=True), (part, 128)
         )
 
-    tick(7)
+    tick(8)
     for copy in stat_copies:
         copy.start()
-    tick(8)
     for copy in stat_copies:
         copy.wait_recv()
 

time: 127 us -> 126 us (level)
  Pallas kernels: 105 us -> 103 us
    pallas_call x1, Pallas kernels: 105 us -> 103 us  [gather_and_project(): pl.pallas_call(functools.partial(gather_kernel, sizes), out_shape=[jax.Sh...]
where the time goes in v3:
time: 126 us; the launch traced here: 125 us
  Pallas kernels  103 us (82%)
  matrix products  9.17 us (7%)
  other arithmetic  6.13 us (5%)
  local copies, waits for them, and re-layouts  4.04 us (3%)
  waiting for transfers between devices  2.65 us (2%)
    pallas_call x1, Pallas kernels, gather_and_project(): pl.pallas_call(functools.partial(gather_kernel, sizes), out_shape=[jax.Sh...  103 us
    dot_general x1, matrix products, local(): jnp.dot(mixer_rows, out_weight, preferred_element_type=jnp.float32)  2.84 us
    ppermute x1, waiting for transfers between devices, sum_groups(): other = lax.ppermute(partial, 'tp', [(0, 1), (1, 0)])  2.65 us
  transfers between devices with their start and end apart: 1, of which 1 were waited for; matrix products, arithmetic and copies ran while one was open for 0% of the time, Pallas kernels for 0%

profile of v3, /device:TPU:0, one launch (start us, length us, event | category | flops | bytes accessed | tf_op | source)
XLA Modules:
  0.0 125.4 jit_solution(11487985203968246603)
XLA Ops:
  0.0 0.1 multiply_cosine_fusion.1
  0.2 0.3 multiply_cosine_fusion
  0.5 1.9 %copy.25.rope_ref = bf16[2048,32]{1,0:T(8,128)(2,1)} copy(bf16[2048,32]{0,1:T(8,128)(2,1)} %param.23) | data formatting | bytes 262144 | tf_op args[4]
  2.4 103.0 %shard_map.181 = (bf16[2,256,384]{2,1,0:T(8,128)(2,1)}, bf16[2,1024,256]{2,1,0:T(8,128)(2,1)}, bf16[1024,32]{1,0:T(8,128)(2,1)}, bf16[256,512]{1,0:T(8,128)(2,1)...) custom-call(bf16[256,2048]{1,0:T(8,128)(2,1)} %bitcast.53, ...), custom_call_target="tpu_custom_call" | custom-call | tf_op jit(solution)/shard_map/pallas_call | solution.py:407
  105.4 0.0 copy-start.1
  105.4 0.0 copy-start
  105.4 0.0 copy-start.5
  105.4 0.0 copy-start.9
  105.4 1.4 %slice_bitcast_fusion.1 = (bf16[1024,256]{1,0:T(8,128)(2,1)S(1)}, bf16[1024,256]{1,0:T(8,128)(2,1)S(1)}) fusion(bf16[2,1024,256]{2,1,0:T(8,128)(2,1)} %get-tuple-element.48), kind=kLoop, calls=%fused_computation.49 | loop fusion | bytes 2097152 | tf_op jit(solution)/shard_map/unstack | solution.py:484
  106.8 0.0 copy-start.2
  106.8 0.3 fusion.13
  107.1 0.0 copy-done.1
  107.1 0.1 copy.26
  107.3 0.0 copy-done
  107.3 0.0 copy-start.7
  107.3 0.0 copy-start.10
  107.3 0.2 fusion.35
  107.5 0.0 copy-done.5
  107.5 0.0 copy-done.9
  107.5 0.6 fusion.41
  108.2 0.1 multiply_reduce_fusion.1
  108.3 0.0 copy-done.2
  108.3 0.0 copy-start.6
  108.3 0.1 multiply_multiply_fusion.1
  108.5 0.0 copy-done.7
  108.5 0.0 copy-done.10
  108.5 0.9 convolution_convert_fusion
  109.4 0.0 copy-done.6
  109.4 0.9 fusion.62
  110.3 0.0 copy-start.3
  110.3 0.1 broadcast_in_dim.91
  110.5 0.4 multiply_reduce_fusion
  110.9 0.1 copy-done.3
  111.0 0.6 multiply_multiply_fusion
  111.6 0.2 slice.52
  111.8 0.2 broadcast_compare_fusion
  112.0 0.1 subtract_convert_fusion
  112.2 1.7 %fusion = (f32[256,8]{0,1:T(8,128)S(1)}, f32[8,1024,256]{2,1,0:T(8,128)S(1)}) fusion(pred[256,1024]{0,1:T(8,128)(4,1)S(1)} %broadcast_compare_fusion, bf16[256,8,16]{0,2,1:T(8,128)(2,1)S(1)} %get-tuple-element.64, bf16[256,8,16]{0,2,1:T(8,128)(2,1)S(1)} %get-tuple-element.63, bf16[256,8,64]{0,2,1:T(8,128)(2,1)S(1)} %slice.53, ...), kind=kOutput, calls=%fused_computation.2 | convolution fusion | flops 414840832 | bytes 10625024 | tf_op jit(solution)/shard_map/while/body/eval_jaxpr/qhd,khd->qhk/dot_general | solution.py:496
  113.9 2.2 %fusion.1 = f32[256,8]{0,1:T(8,128)S(1)} fusion(f32[8,1024,256]{2,1,0:T(8,128)S(1)} %get-tuple-element.74, f32[256,8]{0,1:T(8,128)S(1)} %broadcast_maximum_fusion, pred[256,1024]{0,1:T(8,128)(4,1)S(1)} %broadcast_compare_fusion), kind=kLoop, calls=%fused_computation.3 | loop fusion | flops 10483712 | bytes 8667136 | tf_op jit(solution)/shard_map/while/body/eval_jaxpr/reduce_sum | solution.py:504
  116.1 0.0 copy-start.4
  116.1 0.0 copy-start.8
  116.1 2.2 %fusion.32 = bf16[256,8,64]{0,2,1:T(8,128)(2,1)S(1)} fusion(bf16[1024,8,64]{0,2,1:T(8,128)(2,1)S(1)} %bitcast.58, f32[8,1024,256]{2,1,0:T(8,128)S(1)} %get-tuple-element.74, f32[256,8]{0,1:T(8,128)S(1)} %broadcast_maximum_fusion, pred[256,1024]{0,1:T(8,128)(4,1)S(1)} %broadcast_compare_fusion, f32[256,8]{0,1:T(8,128)S(1)} %get-tuple-element.68, ...), kind=kOutput, calls=%fused_computation.34 | convolution fusion | flops 279314432 | bytes 9986048 | tf_op jit(solution)/shard_map/while/body/eval_jaxpr/qhk,khd->qhd/dot_general | solution.py:505
  118.3 0.1 copy.29
  118.5 0.0 copy-done.4
  118.5 0.0 copy-done.8
  118.5 2.8 %fusion.10 = bf16[256,2048]{1,0:T(8,128)(2,1)S(1)} fusion(bf16[512,2048]{1,0:T(8,128)(2,1)} %get-tuple-element.58, bf16[512,2048]{1,0:T(8,128)(2,1)S(1)} %copy-done.4, bf16[256,512]{1,0:T(8,128)(2,1)S(1)} %copy-done.8, bf16[256,512]{1,0:T(8,128)(2,1)S(1)} %copy.29), kind=kOutput, calls=%fused_computation.16 | convolution fusion | flops 1083703296 | bytes 5767168 | tf_op jit(solution)/shard_map/dot_general | solution.py:547
  121.3 0.1 collective-permute-start
  121.4 2.6 %collective-permute-done = bf16[256,2048]{1,0:T(8,128)(2,1)S(1)} collective-permute-done((bf16[256,2048]{1,0:T(8,128)(2,1)S(1)}, bf16[256,2048]{1,0:T(8,128)(2,1)S(1)}, u32[]{:S(2)}, u32[]{:S(2)}) %collective-permute-start) | collective-permute-done | bytes 1048608 | tf_op jit(solution)/shard_map/ppermute | solution.py:447
  124.1 1.4 %fusion.28 = bf16[1,256,2048]{2,1,0:T(8,128)(2,1)} fusion(bf16[256,2048]{1,0:T(8,128)(2,1)S(1)} %collective-permute-done, bf16[256,2048]{1,0:T(8,128)(2,1)S(1)} %fusion.10), kind=kLoop, calls=%fused_computation.31 | loop fusion | flops 2097152 | bytes 3145728 | tf_op jit(solution)/shard_map/broadcast_in_dim | solution.py:549
  (13 shorter events, 0.2 us)
Async XLA Ops:
  105.4 1.7 %copy-start.1 = (bf16[1024,32]{1,0:T(8,128)(2,1)S(1)}, bf16[1024,32]{1,0:T(8,128)(2,1)}, u32[]{:S(2)}) copy-start(bf16[1024,32]{1,0:T(8,128)(2,1)} %get-tuple-element.52) | copy-start | bytes 196612
  105.4 1.9 %copy-start = (bf16[2,256,384]{2,1,0:T(8,128)(2,1)S(1)}, bf16[2,256,384]{2,1,0:T(8,128)(2,1)}, u32[]{:S(2)}) copy-start(bf16[2,256,384]{2,1,0:T(8,128)(2,1)} %get-tuple-element.53) | copy-start | bytes 1179652
  105.4 2.1 %copy-start.5 = (bf16[768,768]{1,0:T(8,128)(2,1)S(1)}, bf16[768,768]{1,0:T(8,128)(2,1)}, u32[]{:S(2)}) copy-start(bf16[768,768]{1,0:T(8,128)(2,1)} %get-tuple-element.54) | copy-start | bytes 3538948
  105.4 2.1 %copy-start.9 = (f32[768]{0:T(1024)S(1)}, f32[768]{0:T(1024)}, u32[]{:S(2)}) copy-start(f32[768]{0:T(1024)} %param.27) | copy-start | bytes 9220
  106.8 1.4 %copy-start.2 = (f32[96]{0:T(128)S(1)}, f32[96]{0:T(128)}, u32[]{:S(2)}) copy-start(f32[96]{0:T(128)} %param.29) | copy-start | bytes 1156
  107.3 1.2 copy-start.7
  107.3 1.2 copy-start.10
  108.3 1.1 copy-start.6
  110.3 0.7 copy-start.3
  116.1 2.4 %copy-start.4 = (bf16[512,2048]{1,0:T(8,128)(2,1)S(1)}, bf16[512,2048]{1,0:T(8,128)(2,1)}, u32[]{:S(2)}) copy-start(bf16[512,2048]{1,0:T(8,128)(2,1)} %get-tuple-element.57) | copy-start | bytes 6291460
  116.1 2.4 %copy-start.8 = (bf16[256,512]{1,0:T(8,128)(2,1)S(1)}, bf16[256,512]{1,0:T(8,128)(2,1)}, u32[]{:S(2)}) copy-start(bf16[256,512]{1,0:T(8,128)(2,1)} %get-tuple-element.56) | copy-start | bytes 786436
  121.3 2.7 %collective-permute-start = (bf16[256,2048]{1,0:T(8,128)(2,1)S(1)}, bf16[256,2048]{1,0:T(8,128)(2,1)S(1)}, u32[]{:S(2)}, u32[]{:S(2)}) collective-permute-start(bf16[256,2048]{1,0:T(8,128)(2,1)S(1)} %fusion.10), channel_id=1, source_target_pairs={{0,1},{1,0},{2,3},{3,2},{4,5},{5,4},{6,7},{7,6},{8,9},{9,8},{10,11... | collective-permute-start | bytes 3145736 | tf_op jit(solution)/shard_map/ppermute | solution.py:447
